TPU v7x, 256 devices: a whole 4x4x8 slice. The times are simulated.
256 devices in a mesh: rep: 2 (over z_hi), fs: 16 (over z_lo, x), tp: 8 (over y, core).
Axes of the slice: x: 4, y: 4, z: 8 (z_hi: 2, z_lo: 4; z = z_hi * 4 + z_lo), core: 2. Of those that a mesh axis runs over, the one named last changes fastest.
Arguments:
- tokens: bfloat16 [32768, 2048], P(('rep', 'fs', 'tp')), may hold values from -6 to 6
- mix_gain: float32 [2048], replicated, may hold values from 0.1 to 1.9
- w_query: bfloat16 [2048, 1024], P('fs', 'tp'), may hold values from -0.125 to 0.125
- w_key: bfloat16 [2048, 1024], P('fs', 'tp'), may hold values from -0.125 to 0.125
- w_value: bfloat16 [2048, 2048], P('fs', 'tp'), may hold values from -0.125 to 0.125
- w_decay_down: bfloat16 [2048, 32], replicated, may hold values from -0.125 to 0.125
- w_decay_up: bfloat16 [32, 1024], replicated, may hold values from -2 to 2
- decay_bias: float32 [1024], replicated, may hold values from -1 to 6
- decay_shift: float32 [32768, 1024], P(('rep', 'fs'), 'tp'), may hold values from -3 to 0
- head_gain: float32 [2048], replicated, may hold values from 0.1 to 1.9
- w_mix_out: bfloat16 [2048, 2048], P('tp', 'fs'), may hold values from -0.125 to 0.125
- ffn_gain: float32 [2048], replicated, may hold values from 0.1 to 1.9
- w_gate: bfloat16 [2048, 5632], P('fs', 'tp'), may hold values from -0.125 to 0.125
- w_up: bfloat16 [2048, 5632], P('fs', 'tp'), may hold values from -0.125 to 0.125
- w_down: bfloat16 [5632, 2048], P('tp', 'fs'), may hold values from -0.078125 to 0.078125
Outputs:
- layer_out: float32 [32768, 2048], P(('rep', 'fs', 'tp'))
All inputs are finite; a program needn't handle non-finite values.
Results may differ from a plain program's by a relative error of at most 0.04.
Values may be sent and summed in bfloat16 or wider, within the bound.
A program may use at most 128 MiB of HBM per device.

v0:
```python
import jax
import jax.numpy as jnp
from jax import lax
from jax.sharding import Mesh
from jax.sharding import PartitionSpec as P

KEY_CHANNELS = 128
DV = 256
BLK = 64
FS = ("fs_0", "fs_1")
REP_FS_TP = ("rep", "fs_0", "fs_1", "tp")
REP_FS = ("rep", "fs_0", "fs_1")


EPS = 1e-06
TAU = 16.0


def sent_together(arrays, axis, dim, along):
    widths = [a.shape[along] for a in arrays]
    both = jnp.concatenate(arrays, axis=along)
    whole = lax.all_gather(both, axis, axis=dim, tiled=True)
    return tuple(jnp.split(whole, [sum(widths[:k]) for k in range(1, len(widths))], axis=along))


def in_order(pieces, dim):
    shape = list(pieces.shape[1:])
    shape[dim] *= pieces.shape[0]
    return jnp.moveaxis(pieces, 0, dim).reshape(shape)


def copy_for_each(value, axis):
    copies = jnp.broadcast_to(value, (lax.axis_size(axis), *value.shape))
    return lax.all_to_all(copies, axis, split_axis=0, concat_axis=0, tiled=True)


def collect(value, axis, dim):
    return in_order(copy_for_each(value, axis), dim)


def cut_along(value, dim, size):
    shape = value.shape
    pieces = value.reshape(*shape[:dim], size, shape[dim] // size, *shape[dim + 1 :])
    return jnp.moveaxis(pieces, dim, 0)


def sent_and_summed(value, axis, dim):
    pieces = cut_along(value, dim, lax.axis_size(axis))
    arrived = lax.all_to_all(pieces, axis, split_axis=0, concat_axis=0, tiled=True)
    return arrived.astype(jnp.float32).sum(axis=0)


def stacked_from(value, axes, turns):
    pieces = value
    for k in turns:
        pieces = lax.all_gather(pieces, axes[k])
    done = turns[::-1]
    back = [done.index(k) for k in range(len(axes))]
    pieces = pieces.transpose(*back, *range(len(axes), pieces.ndim))
    return pieces.reshape(-1, *value.shape)


def whole_of(value, axes, turns, dim):
    return in_order(stacked_from(value, axes, turns), dim)


def rms_norm(values, gain):
    return values * lax.rsqrt(jnp.mean(values * values, axis=-1, keepdims=True) + EPS) * gain


def recurrence(query_proj, key_proj, value_proj, log_decay, head_count):
    seq_rows = query_proj.shape[0]
    blocks = seq_rows // BLK
    queries = query_proj.astype(jnp.float32).reshape(
        blocks, BLK, head_count, KEY_CHANNELS
    ) * KEY_CHANNELS ** (-0.5)
    keys = key_proj.astype(jnp.float32).reshape(blocks, BLK, head_count, KEY_CHANNELS)
    values = value_proj.astype(jnp.float32).reshape(blocks, BLK, head_count, DV)
    decays = log_decay.reshape(blocks, BLK, head_count, KEY_CHANNELS)
    cumul = jnp.cumsum(decays, axis=1)
    totals = cumul[:, -1]
    weighted = keys * jnp.exp(totals[:, None] - cumul)
    updates = jnp.einsum("bchd,bche->bhde", weighted, values)

    def combine(earlier, later):
        return (earlier[0] + later[0], jnp.exp(later[0])[..., None] * earlier[1] + later[1])

    _, states = lax.associative_scan(combine, (totals, updates), axis=0)
    previous = jnp.concatenate([jnp.zeros_like(states[:1]), states[:-1]], axis=0)
    q_decayed = queries * jnp.exp(cumul)
    k_decayed = keys * jnp.exp(-cumul)
    scores = jnp.einsum("bchd,bshd->bhcs", q_decayed, k_decayed)
    causal = (jnp.arange(BLK)[:, None] >= jnp.arange(BLK)[None, :]).astype(jnp.float32)
    scores = scores * causal
    inner = jnp.einsum("bhcs,bshe->bche", scores, values)
    carried = jnp.einsum("bchd,bhde->bche", q_decayed, previous)
    return (inner + carried).reshape(seq_rows, head_count, DV)


def per_device(
    tokens,
    mix_gain,
    w_query,
    w_key,
    w_value,
    w_decay_down,
    w_decay_up,
    decay_bias,
    decay_shift,
    head_gain,
    w_mix_out,
    ffn_gain,
    w_gate,
    w_up,
    w_down,
):
    tp_index = lax.axis_index("tp")
    key_cols = w_query.shape[1]
    value_cols = w_value.shape[1]
    heads_dev = key_cols // KEY_CHANNELS
    own_rows = tokens.astype(jnp.float32)
    normed = lax.all_gather(
        rms_norm(own_rows, mix_gain).astype(jnp.bfloat16), "tp", axis=0, tiled=True
    )
    seq_rows = normed.shape[0]
    pieces = sent_together((w_query, w_key, w_value), FS, 0, 1)
    first = jnp.dot(normed, pieces[0], preferred_element_type=jnp.float32)
    second = jnp.dot(normed, pieces[1], preferred_element_type=jnp.float32)
    third = jnp.dot(normed, pieces[2], preferred_element_type=jnp.float32)
    query_proj = first.astype(jnp.bfloat16)
    key_proj = second.astype(jnp.bfloat16)
    value_proj = third.astype(jnp.bfloat16)
    low_rank = jnp.dot(normed, w_decay_down, preferred_element_type=jnp.float32).astype(
        jnp.bfloat16
    )
    up_columns = lax.dynamic_slice_in_dim(w_decay_up, tp_index * key_cols, key_cols, 1)
    bias_columns = lax.dynamic_slice_in_dim(decay_bias, tp_index * key_cols, key_cols, 0)
    pre_decay = jnp.dot(low_rank, up_columns, preferred_element_type=jnp.float32) + bias_columns
    log_decay = jax.nn.log_sigmoid(pre_decay) / TAU + decay_shift
    head_out = recurrence(query_proj, key_proj, value_proj, log_decay, heads_dev)
    gain_columns = lax.dynamic_slice_in_dim(head_gain, tp_index * value_cols, value_cols, 0)
    gated = rms_norm(head_out, gain_columns.reshape(heads_dev, DV)).astype(jnp.bfloat16)
    gated = gated.reshape(seq_rows, value_cols)
    out_weight = collect(w_mix_out, FS, 1)
    rows_part = gated
    hidden = own_rows + sent_and_summed(
        jnp.dot(rows_part, out_weight, preferred_element_type=jnp.float32).astype(jnp.bfloat16),
        "tp",
        0,
    )
    normed_ffn = lax.all_gather(
        rms_norm(hidden, ffn_gain).astype(jnp.bfloat16), "tp", axis=0, tiled=True
    )

    def add_single(piece):
        return jnp.dot(normed_ffn, piece, preferred_element_type=jnp.float32)

    gate_proj = add_single(whole_of(w_gate, FS, (0, 1), 0))
    up_proj = add_single(whole_of(w_up, FS, (0, 1), 0))
    activated = (jax.nn.silu(gate_proj) * up_proj).astype(jnp.bfloat16)
    down_weight = whole_of(w_down, FS, (0, 1), 1)
    rows_part = activated
    return hidden + sent_and_summed(
        jnp.dot(rows_part, down_weight, preferred_element_type=jnp.float32).astype(jnp.bfloat16),
        "tp",
        0,
    )


def solution(mesh):
    finer = Mesh(
        mesh.devices.reshape(mesh.shape["rep"], 4, 4, mesh.shape["tp"]),
        ("rep", "fs_0", "fs_1", "tp"),
    )
    return jax.shard_map(
        per_device,
        mesh=finer,
        in_specs=(
            P(REP_FS_TP, None),
            P(),
            P(FS, "tp"),
            P(FS, "tp"),
            P(FS, "tp"),
            P(),
            P(),
            P(),
            P(REP_FS, "tp"),
            P(),
            P("tp", FS),
            P(),
            P(FS, "tp"),
            P(FS, "tp"),
            P("tp", FS),
        ),
        out_specs=P(REP_FS_TP, None),
        check_vma=False,
    )
```

profile of v0, /device:TPU:1, one launch (start us, length us, event | category | flops | bytes accessed | tf_op | source)
XLA Modules:
  0.0 375.4 jit_solution(6054511233803079239)
XLA Ops:
  6.5 1.3 fusion.8
  7.8 2.0 fusion.10
  9.9 1.5 pad_maximum_fusion.3
  11.5 17.8 %all-gather = bf16[512,704]{0,1:T(8,128)(2,1)S(1)} all-gather(bf16[128,704]{0,1:T(8,128)(2,1)} %param.27), channel_id=2, replica_groups=mesh['rep'=2,'fs_0'=4,'fs_1'=4,'tp'=8] {'fs_0'}, dimensions={0}, use_global_device_ids=true | all-gather | bytes 901120 | tf_op jit(solution)/shard_map/all_gather | solution.py:56
  29.3 1.0 copy_bitcast_fusion.1
  30.4 1.1 broadcast_in_dim.2
  31.5 6.3 %all-to-all-start = ((bf16[16,256,128]{1,2,0:T(8,128)(2,1)}), bf16[16,256,128]{1,2,0:T(8,128)(2,1)}, u32[]{:S(2)}, u32[]{:S(2)}) async-start(bf16[16,256,128]{1,2,0:T(8,128)(2,1)} %broadcast_in_dim.2), calls=%async_computation | async-start | bytes 2097152 | tf_op jit(solution)/shard_map/all_to_all | solution.py:34
  37.9 45.2 %all-gather.2 = bf16[512,704]{0,1:T(8,128)(2,1)S(1)} all-gather(bf16[128,704]{0,1:T(8,128)(2,1)S(1)} %copy-done.13), channel_id=4, replica_groups=mesh['rep'=2,'fs_0'=4,'fs_1'=4,'tp'=8] {'fs_0'}, dimensions={0}, use_global_device_ids=true | all-gather | bytes 901120 | tf_op jit(solution)/shard_map/all_gather | solution.py:56
  83.1 1.0 copy_bitcast_fusion
  84.2 0.6 fusion.43
  84.8 0.8 dynamic_slice.10
  85.5 0.8 dynamic_slice.11
  86.3 3.9 %fusion.18 = f32[1024,128]{1,0:T(8,128)S(1)} fusion(f32[1024,128]{1,0:T(8,128)S(1)} %copy-done.11, bf16[1024,2048]{1,0:T(8,128)(2,1)} %all-gather.13.cloned.1.call-done, bf16[2048,32]{0,1:T(8,128)(2,1)S(1)} %copy-done, f32[128]{0:T(128)S(1)} %dynamic_slice.10, bf16[32,1024]{1,0:T(8,128)(2,1)} %param.21, s32[]{:T(128)S(6)} %select_n.12), kind=kOutput, calls=%fused_computation.42 | convolution fusion | flops 144080896 | bytes 5382660 | tf_op jit(solution)/shard_map/dot_general | solution.py:138
  90.2 0.3 fusion.30
  90.6 0.5 exponential_bitcast_fusion.6
  91.2 33.2 %all-gather.15.cloned.1.call-done = bf16[2048,512]{1,0:T(8,128)(2,1)} async-done(((bf16[128,512]{1,0:T(8,128)(2,1)}), bf16[2048,512]{1,0:T(8,128)(2,1)}) %all-gather.15.cloned.1.call-update) | async-done | bytes 2097168 | tf_op jit(solution)/shard_map/all_gather | solution.py:22
  124.5 3.7 convolution_convert_fusion.3
  128.2 0.5 copy-done.18
  128.8 1.2 fusion.7
  130.0 1.5 fusion.23
  131.5 1.2 convolution_convert_fusion.2
  132.8 0.5 fusion.26
  133.2 0.3 copy-done.7
  133.9 0.8 copy-done.6
  134.7 0.8 slice_add_fusion.2
  135.6 0.7 slice.128
  136.2 1.1 fusion.49
  137.3 0.7 copy-done.9
  138.0 1.1 fusion.48
  139.0 0.7 pad_maximum_fusion.2
  139.8 2.4 pad.28
  142.2 1.6 pad_add_fusion
  143.8 2.5 pad.29
  146.3 2.2 add.145
  148.5 1.2 fusion.38
  149.7 0.8 pad_maximum_fusion.1
  150.6 2.0 pad.30
  152.5 4.1 %pad.31 = f32[8,1,128,256]{3,2,0,1:T(8,128)} pad(f32[4,1,128,256]{3,2,0,1:T(8,128)} %add.145, f32[]{:T(128)} %constant.13.clone.1), padding=1_0_1x0_0_0x0_0_0x0_0_0 | pad | bytes 1572868 | tf_op jit(solution)/shard_map/pad | solution.py:88
  156.7 2.4 add.147
  159.1 0.3 fusion.13
  159.5 4.0 %pad.44 = f32[15,1,128,256]{3,2,0,1:T(8,128)} pad(f32[8,1,128,256]{3,2,0,1:T(8,128)S(1)} %pad_maximum_fusion, f32[]{:T(128)} %constant.13.clone.1), padding=0_0_1x0_0_0x0_0_0x0_0_0 | pad | bytes 3014660 | tf_op jit(solution)/shard_map/slice | solution.py:89
  163.5 0.2 pad.67
  163.8 1.9 slice_add_fusion.4
  165.6 0.3 fusion.2
  166.0 0.5 fusion.12
  166.5 4.5 %convolution_convert_fusion.1 = bf16[1024,2048]{1,0:T(8,128)(2,1)} fusion(bf16[256,2048]{0,1:T(8,128)(2,1)} %bitcast.24, f32[1024,1,1,1,1,1,256]{6,0,5,4,3,2,1:T(8,128)S(1)} %bitcast.105, f32[256]{0:T(256)S(1)} %dynamic_slice.11, f32[1024]{0:T(1024)S(1)} %rsqrt.29), kind=kOutput, calls=%fused_computation.3 | convolution fusion | flops 1076625408 | bytes 6296576 | tf_op jit(solution)/shard_map/dot_general | solution.py:147
  171.1 15.0 %all-to-all-start.1 = ((bf16[8,128,2048]{2,1,0:T(8,128)(2,1)}), bf16[8,128,2048]{2,1,0:T(8,128)(2,1)}, u32[]{:S(2)}, u32[]{:S(2)}) async-start(bf16[8,128,2048]{2,1,0:T(8,128)(2,1)} %bitcast.102), calls=%async_computation.1 | async-start | bytes 8388608 | tf_op jit(solution)/shard_map/all_to_all | solution.py:49
  186.1 15.4 %all-gather.4 = bf16[2816,128]{1,0:T(8,128)(2,1)} all-gather(bf16[704,128]{1,0:T(8,128)(2,1)S(1)} %copy-done.14), channel_id=6, replica_groups=mesh['rep'=2,'fs_0'=4,'fs_1'=4,'tp'=8] {'fs_0'}, dimensions={0}, use_global_device_ids=true | all-gather | bytes 901120 | tf_op jit(solution)/shard_map/all_gather | solution.py:56
  201.5 0.2 all-gather.17.cloned.1.call-start
  201.7 33.1 %all-to-all-done.1 = bf16[8,128,2048]{2,1,0:T(8,128)(2,1)} async-done(((bf16[8,128,2048]{2,1,0:T(8,128)(2,1)}), bf16[8,128,2048]{2,1,0:T(8,128)(2,1)}, u32[]{:S(2)}, u32[]{:S(2)}) %all-to-all-start.1) | async-done | bytes 4194336 | tf_op jit(solution)/shard_map/all_to_all | solution.py:49
  234.9 3.0 convert_reduce_fusion.1
  237.9 0.2 multiply_reduce_fusion
  238.2 1.0 multiply_convert_fusion.1
  239.2 5.6 %copy.68 = bf16[4,4,128,704]{2,1,0,3:T(4,128)(2,1)} copy(bf16[4,4,128,704]{2,3,0,1:T(8,128)(2,1)} %bitcast.107) | data formatting | bytes 5767168 | tf_op jit(solution)/shard_map/transpose | solution.py:59
  244.8 5.7 %reshape_reshape.6 = bf16[2048,704]{0,1:T(8,128)(2,1)} reshape(bf16[4,4,128,704]{2,1,0,3:T(4,128)(2,1)} %copy.68) | data formatting | bytes 5767168 | tf_op jit(solution)/shard_map/reshape;reshape | solution.py:29
  250.6 5.6 %copy.70 = bf16[4,4,128,704]{2,1,0,3:T(4,128)(2,1)} copy(bf16[4,4,128,704]{2,3,0,1:T(8,128)(2,1)} %bitcast.108) | data formatting | bytes 5767168 | tf_op jit(solution)/shard_map/transpose | solution.py:59
  256.2 5.8 %reshape_reshape.7 = bf16[2048,704]{0,1:T(8,128)(2,1)} reshape(bf16[4,4,128,704]{2,1,0,3:T(4,128)(2,1)} %copy.70) | data formatting | bytes 5767168 | tf_op jit(solution)/shard_map/reshape;reshape | solution.py:29
  262.0 3.6 copy.71
  265.5 28.8 %all-gather.17.cloned.1.call-done = bf16[1024,2048]{1,0:T(8,128)(2,1)} async-done(((bf16[128,2048]{1,0:T(8,128)(2,1)}), bf16[1024,2048]{1,0:T(8,128)(2,1)}) %all-gather.17.cloned.1.call-update) | async-done | bytes 4194320 | tf_op jit(solution)/shard_map/all_gather | solution.py:151
  294.3 7.9 %fusion.57 = f32[1024,704]{0,1:T(8,128)} fusion(bf16[1024,2048]{1,0:T(8,128)(2,1)} %all-gather.17.cloned.1.call-done, bf16[2048,704]{0,1:T(8,128)(2,1)} %reshape_reshape.6), kind=kOutput, calls=%fused_computation.103 | convolution fusion | flops 2952790016 | bytes 9961472 | tf_op jit(solution)/shard_map/dot_general | solution.py:156
  302.2 12.0 %convolution_convert_fusion = bf16[1024,2048]{1,0:T(8,128)(2,1)} fusion(bf16[16,88,8,128]{3,2,1,0:T(8,128)(2,1)} %bitcast.110, f32[1024,704]{0,1:T(8,128)} %fusion.57, bf16[1024,2048]{1,0:T(8,128)(2,1)} %all-gather.17.cloned.1.call-done, bf16[2048,704]{0,1:T(8,128)(2,1)} %reshape_reshape.7), kind=kOutput, calls=%fused_computation.2 | convolution fusion | flops 5912002560 | bytes 17039360 | tf_op jit(solution)/shard_map/dot_general | solution.py:164
  314.2 52.5 %all_to_all.15 = bf16[8,128,2048]{2,1,0:T(8,128)(2,1)S(1)} all-to-all(bf16[8,128,2048]{2,1,0:T(8,128)(2,1)} %bitcast.106), channel_id=1, replica_groups=mesh['rep'=2,'fs_0'=4,'fs_1'=4,'tp'=8] {'tp'}, dimensions={0} | all-to-all | bytes 8388608 | tf_op jit(solution)/shard_map/all_to_all | solution.py:49
  366.7 0.7 convert_reduce_fusion
  367.4 1.1 fusion.37
  (75 shorter events, 1.2 us)
Async XLA Ops:
  6.5 79.8 %copy-start = (bf16[2048,32]{0,1:T(8,128)(2,1)S(1)}, bf16[2048,32]{0,1:T(8,128)(2,1)}, u32[]{:S(2)}) copy-start(bf16[2048,32]{0,1:T(8,128)(2,1)} %param.20) | copy-start | bytes 393220
  6.5 23.8 %copy-start.16 = (bf16[256,128]{1,0:T(8,128)(2,1)S(1)}, bf16[256,128]{1,0:T(8,128)(2,1)}, u32[]{:S(2)}) copy-start(bf16[256,128]{1,0:T(8,128)(2,1)} %param.25) | copy-start | bytes 196612
  6.5 79.7 %all-gather.13.cloned.1.call-start = ((), (), s32[]{:S(2)}) async-start(), calls=%async_computation.3 | async-start | bytes 4718592 | tf_op jit(solution)/shard_map/all_gather | solution.py:122
  9.9 114.6 %all-gather.15.cloned.1.call-start = ((), (), s32[]{:S(2)}) async-start(), calls=%async_computation.4 | async-start | bytes 2228224 | tf_op jit(solution)/shard_map/all_gather | solution.py:22
  11.5 227.7 %all-gather.19.cloned.1.call-start = ((), (), s32[]{:S(2)}) async-start(), calls=%async_computation.6 | async-start | bytes 3604480 | tf_op jit(solution)/shard_map/all_gather | solution.py:56
  29.3 8.6 %copy-start.13 = (bf16[128,704]{0,1:T(8,128)(2,1)S(1)}, bf16[128,704]{0,1:T(8,128)(2,1)}, u32[]{:S(2)}) copy-start(bf16[128,704]{0,1:T(8,128)(2,1)} %param.28) | copy-start | bytes 540676
  31.5 54.8 %copy-start.11 = (f32[1024,128]{1,0:T(8,128)S(1)}, f32[1024,128]{1,0:T(8,128)}, u32[]{:S(2)}) copy-start(f32[1024,128]{1,0:T(8,128)} %param.23) | copy-start | bytes 1572868
  31.5 135.0 %all-to-all-start = ((bf16[16,256,128]{1,2,0:T(8,128)(2,1)}), bf16[16,256,128]{1,2,0:T(8,128)(2,1)}, u32[]{:S(2)}, u32[]{:S(2)}) async-start(bf16[16,256,128]{1,2,0:T(8,128)(2,1)} %broadcast_in_dim.2), calls=%async_computation | async-start | bytes 2097152 | tf_op jit(solution)/shard_map/all_to_all | solution.py:34
  37.9 212.7 %all-gather.21.cloned.1.call-start = ((), (), s32[]{:S(2)}) async-start(), calls=%async_computation.7 | async-start | bytes 3604480 | tf_op jit(solution)/shard_map/all_gather | solution.py:56
  124.4 3.8 %copy-start.5 = (bf16[1024,2048]{1,0:T(8,128)(2,1)S(1)}, bf16[1024,2048]{1,0:T(8,128)(2,1)}, u32[]{:S(2)}) copy-start(bf16[1024,2048]{1,0:T(8,128)(2,1)} %all-gather.13.cloned.1.call-done) | copy-start | bytes 12582916
  124.4 4.3 %copy-start.18 = (bf16[2048,512]{1,0:T(8,128)(2,1)S(1)}, bf16[2048,512]{1,0:T(8,128)(2,1)}, u32[]{:S(2)}) copy-start(bf16[2048,512]{1,0:T(8,128)(2,1)} %all-gather.15.cloned.1.call-done) | copy-start | bytes 6291460
  132.7 0.8 copy-start.7
  133.9 0.8 copy-start.6
  137.3 0.7 copy-start.9
  143.8 5.9 %copy-start.12 = (f32[1,1,128,256]{3,2,0,1:T(8,128)S(1)}, f32[1,1,128,256]{3,2,0,1:T(8,128)}, u32[]{:S(2)}) copy-start(f32[1,1,128,256]{3,2,0,1:T(8,128)} %slice.128) | copy-start | bytes 393220
  156.7 2.5 copy-start.3
  159.4 4.1 %copy-start.4 = (f32[8,1,128,256]{3,2,0,1:T(8,128)S(1)}, f32[8,1,128,256]{3,2,0,1:T(8,128)}, u32[]{:S(2)}) copy-start(f32[8,1,128,256]{3,2,0,1:T(8,128)} %add.147) | copy-start | bytes 3145732
  163.7 2.2 copy-start.8
  163.8 2.2 copy-start.10
  163.8 2.2 copy-start.15
  171.1 15.0 %copy-start.14 = (bf16[704,128]{1,0:T(8,128)(2,1)S(1)}, bf16[704,128]{1,0:T(8,128)(2,1)}, u32[]{:S(2)}) copy-start(bf16[704,128]{1,0:T(8,128)(2,1)} %param.29) | copy-start | bytes 540676
  171.1 63.8 %all-to-all-start.1 = ((bf16[8,128,2048]{2,1,0:T(8,128)(2,1)}), bf16[8,128,2048]{2,1,0:T(8,128)(2,1)}, u32[]{:S(2)}, u32[]{:S(2)}) async-start(bf16[8,128,2048]{2,1,0:T(8,128)(2,1)} %bitcast.102), calls=%async_computation.1 | async-start | bytes 8388608 | tf_op jit(solution)/shard_map/all_to_all | solution.py:49
  186.1 75.9 %all-gather.23.cloned.1.call-start = ((), (), s32[]{:S(2)}) async-start(), calls=%async_computation.8 | async-start | bytes 3604480 | tf_op jit(solution)/shard_map/all_gather | solution.py:56
  201.5 36.4 %copy-start.2 = (bf16[128,2048]{1,0:T(8,128)(2,1)S(1)}, bf16[128,2048]{1,0:T(8,128)(2,1)}, u32[]{:S(2)}) copy-start(bf16[128,2048]{1,0:T(8,128)(2,1)} %param.15) | copy-start | bytes 1572868
  201.5 36.7 %copy-start.17 = (f32[2048]{0:T(1024)S(1)}, f32[2048]{0:T(1024)}, u32[]{:S(2)}) copy-start(f32[2048]{0:T(1024)} %param.26) | copy-start | bytes 24580
  201.5 92.8 %all-gather.17.cloned.1.call-start = ((), (), s32[]{:S(2)}) async-start(), calls=%async_computation.5 | async-start | bytes 4718592 | tf_op jit(solution)/shard_map/all_gather | solution.py:151
  366.7 1.9 copy-start.1
Sparse Core Ops, SparseCore 0:
  10.0 38.8 all-gather.12
  50.6 73.7 all-gather.14
  126.3 47.4 all-gather.18
  175.4 40.0 all-gather.20
  217.1 40.0 all-gather.22
  258.9 35.3 all-gather.16
where the time goes:
time: 377 us; the launch traced here: 375 us
  blocking collectives  131 us (35%)
  waiting for transfers between devices  95.3 us (25%)
  local copies, waits for them, and re-layouts  50 us (13%)
  matrix products  35.8 us (9%)
  other arithmetic  27.9 us (7%)
  starting transfers between devices  21.7 us (6%)
  between operations  13.8 us (4%)
    all_gather x3, blocking collectives, stacked_from(): pieces = lax.all_gather(pieces, axes[k])  78.4 us
    all_to_all x1, blocking collectives, sent_and_summed(): lax.all_to_all(pieces, axis, split_axis=0, concat_axis=0, tiled=True)  52.5 us
    all_gather x1, waiting for transfers between devices, sent_together(): whole = lax.all_gather(both, axis, axis=dim, tiled=True)  33.2 us
    all_to_all x1, waiting for transfers between devices, sent_and_summed(): lax.all_to_all(pieces, axis, split_axis=0, concat_axis=0, tiled=True)  33.1 us
    all_gather x1, waiting for transfers between devices, per_device(): lax.all_gather(rms_norm(hidden, ffn_gain).astype(jnp.bfloat16), 'tp', axi...  28.8 us
    all_to_all x1, starting transfers between devices, sent_and_summed(): lax.all_to_all(pieces, axis, split_axis=0, concat_axis=0, tiled=True)  15 us
    transpose x3, local copies, waits for them, and re-layouts, stacked_from(): pieces = pieces.transpose(*back, *range(len(axes), pieces.ndim))  14.8 us
    dot_general x1, matrix products, per_device(): jnp.dot(rows_part, down_weight, preferred_element_type=jnp.float32)  12 us
  transfers between devices with their start and end apart: 8, of which 3 were waited for; matrix products, arithmetic and copies ran while one was open for 23% of the time, Pallas kernels for 0%

commit v1 on v0

v1 whole, which is shorter than its diff:
```python
import jax
import jax.numpy as jnp
from jax import lax
from jax.experimental import pallas as pl
from jax.experimental.pallas import tpu as pltpu
from jax.sharding import Mesh
from jax.sharding import PartitionSpec as P

AXES = ("rep", "fz", "fx", "ty", "tc")
MESH = pl.DeviceIdType.MESH
KEY_CHANNELS = 128
DV = 256
BLK = 64
EPS = 1e-06
TAU = 16.0
F32 = jnp.float32
BF16 = jnp.bfloat16
QKV, OUT, GATE, UP, DOWN = range(5)


def rms_norm(values, gain):
    return values * lax.rsqrt(jnp.mean(values * values, axis=-1, keepdims=True) + EPS) * gain


def dot(a, b, dims=(((1,), (0,)), ((), ()))):
    return lax.dot_general(a, b, dims, preferred_element_type=F32)


def order(i):
    return jnp.where(i < 2, i, 5 - i)


def kernel(
    tokens_hbm, shift_hbm, wq_hbm, wk_hbm, wv_hbm, wo_hbm, wg_hbm, wu_hbm, wd_hbm,
    mix_gain, ffn_gain, head_gain, down_proj, up_proj, bias,
    out,
    wqkv, wo, wg, wu, wd,
    tok, shift, n1, n2, qs, ks, vs, gated, state, hidden, act,
    keep1, send1, cross1, recv1, keep2, send2, cross2, recv2,
    loc_sem, w_send, w_recv,
    ag1_send, ag1_recv, ag2_send, ag2_recv,
    x1_send, x1_recv, r1_send, r1_recv, x2_send, x2_recv, r2_send, r2_recv,
):
    rep, fz, fx = lax.axis_index("rep"), lax.axis_index("fz"), lax.axis_index("fx")
    ty, tc = lax.axis_index("ty"), lax.axis_index("tc")
    tp = ty * 2 + tc
    weights = (wqkv, wo, wg, wu, wd)

    def at_x(k):
        return {"fx": lax.rem(fx + k, 4)}

    def at_z(k):
        whole = lax.rem(rep * 4 + fz + k + 8, 8)
        return {"rep": whole // 4, "fz": lax.rem(whole, 4)}

    def at_y(k):
        return {"ty": lax.rem(ty + k, 4)}

    other = {"tc": 1 - tc}

    mine = [
        pltpu.make_async_copy(tokens_hbm, tok, loc_sem.at[0]),
        pltpu.make_async_copy(wq_hbm, wqkv.at[fz, fx, :, :, pl.ds(0, 128)], loc_sem.at[1]),
        pltpu.make_async_copy(wk_hbm, wqkv.at[fz, fx, :, :, pl.ds(128, 128)], loc_sem.at[2]),
        pltpu.make_async_copy(wv_hbm, wqkv.at[fz, fx, :, :, pl.ds(256, 256)], loc_sem.at[3]),
        pltpu.make_async_copy(wo_hbm, wo.at[fz, fx], loc_sem.at[4]),
        pltpu.make_async_copy(wg_hbm, wg.at[fz, fx], loc_sem.at[5]),
        pltpu.make_async_copy(wu_hbm, wu.at[fz, fx], loc_sem.at[6]),
        pltpu.make_async_copy(wd_hbm, wd.at[fz, fx], loc_sem.at[7]),
        pltpu.make_async_copy(shift_hbm, shift, loc_sem.at[8]),
    ]
    for copy in mine:
        copy.start()

    barrier = pltpu.get_barrier_semaphore()
    peers = [at_x(1), at_x(2), at_x(3), at_z(1), at_z(-1), at_z(2), at_z(-2), at_y(1), at_y(2), at_y(3), other]
    for peer in peers:
        pl.semaphore_signal(barrier, inc=1, device_id=peer, device_id_type=MESH)

    mine[0].wait()
    n1[ty, tc] = rms_norm(tok[...].astype(F32), mix_gain[...]).astype(BF16)
    for copy in mine[1:8]:
        copy.wait()

    pl.semaphore_wait(barrier, len(peers))

    pending = []

    def push(src, dst, send, recv, peer):
        copy = pltpu.make_async_remote_copy(
            src_ref=src, dst_ref=dst, send_sem=send, recv_sem=recv, device_id=peer, device_id_type=MESH
        )
        copy.start()
        return copy

    def spread(buf, z, x, first, count, g, phase, peer):
        piece = buf.at[z, x, pl.ds(first, count)]
        push(piece, piece, w_send.at[g, phase], w_recv.at[g, phase], peer)

    def first_phase(g):
        buf = weights[g]
        for k in (1, 3, 2):
            spread(buf, fz, fx, 0, 2, g, 0, at_x(k))
        for k in (1, -1):
            spread(buf, fz, fx, 2, 2, g, 1, at_z(k))
        spread(buf, fz, fx, 2, 1, g, 1, at_z(2))
        spread(buf, fz, fx, 3, 1, g, 1, at_z(-2))

    def three(buf):
        return buf.at[0, pl.ds(0, 3), pl.ds(0, 2)]

    def twelve(buf):
        return buf.at[pl.ds(0, 3), :, pl.ds(0, 2)]

    def await_bytes(view, sem):
        pltpu.make_async_copy(view, view, sem).wait()

    def second_phase(g):
        buf = weights[g]
        await_bytes(three(buf), w_recv.at[g, 0])
        await_bytes(three(buf), w_recv.at[g, 1])
        every = slice(None)
        for k in (1, -1):
            spread(buf, fz, every, 0, 2, g, 2, at_z(k))
        spread(buf, fz, every, 0, 1, g, 2, at_z(2))
        spread(buf, fz, every, 1, 1, g, 2, at_z(-2))
        for k in (1, 3, 2):
            spread(buf, every, fx, 2, 2, g, 3, at_x(k))

    def arrived(g):
        buf = weights[g]
        await_bytes(twelve(buf), w_recv.at[g, 2])
        await_bytes(twelve(buf), w_recv.at[g, 3])

    def gather_start(buf, send, recv):
        own = buf.at[ty, tc]
        for j, peer in enumerate((other, at_y(1), at_y(3), at_y(2))):
            push(own, own, send.at[j], recv.at[tp], peer)

    def gather_next(buf, send, recv, i):
        chip = lax.rem(ty + order(i), 4)
        mine_slot, theirs = buf.at[chip, tc], buf.at[chip, 1 - tc]

        @pl.when(i > 0)
        def _():
            await_bytes(mine_slot, recv.at[chip * 2 + tc])
            push(mine_slot, mine_slot, send.at[3 + i], recv.at[chip * 2 + tc], other)

        await_bytes(theirs, recv.at[chip * 2 + 1 - tc])
        return chip

    def gather_finish(buf, send):
        for j in range(7):
            await_bytes(buf.at[0, 0], send.at[j])

    def cross_start(chip, parts, send_buf, cross_buf, send, recv):
        push(send_buf.at[chip], cross_buf.at[chip], send.at[chip], recv.at[chip], other)

    def scatter_send(chip, keep, cross_buf, recv_buf, x_recv, r_send, r_recv):
        await_bytes(cross_buf.at[chip], x_recv.at[chip])
        keep[chip] = (keep[chip].astype(F32) + cross_buf[chip].astype(F32)).astype(BF16)
        push(keep.at[chip], recv_buf.at[ty], r_send.at[chip], r_recv.at[ty], {"ty": chip})

    gather_start(n1, ag1_send, ag1_recv)
    first_phase(QKV)
    first_phase(OUT)
    first_phase(GATE)
    second_phase(QKV)
    second_phase(OUT)
    first_phase(UP)
    first_phase(DOWN)

    mine[8].wait()

    arrived(QKV)

    @pl.loop(0, 4)
    def project(i):
        chip = gather_next(n1, ag1_send, ag1_recv, i)
        rows = pl.ds(pl.multiple_of(chip * 256, 256), 256)
        x = n1[chip].reshape(256, 2048)
        both = dot(x, wqkv[:, :, :, :, pl.ds(0, 256)].reshape(2048, 256))
        qs[rows, :] = both[:, :128].astype(BF16)
        ks[rows, :] = both[:, 128:].astype(BF16)
        vs[rows, :] = dot(x, wqkv[:, :, :, :, pl.ds(256, 256)].reshape(2048, 256)).astype(BF16)
        low = dot(x, down_proj[...]).astype(BF16)
        cols = pl.ds(pl.multiple_of(tp * 128, 128), 128)
        pre = dot(low, up_proj[:, cols]) + bias[:, cols]
        soft = jnp.minimum(pre, 0.0) - jnp.log1p(jnp.exp(-jnp.abs(pre)))
        shift[rows, :] = soft / TAU + shift[rows, :]

    second_phase(GATE)

    ri = lax.broadcasted_iota(jnp.int32, (128, 128), 0)
    ci = lax.broadcasted_iota(jnp.int32, (128, 128), 1)
    causal = jnp.where((ri >= ci) & (ri // BLK == ci // BLK), 1.0, 0.0).astype(F32)
    state[...] = jnp.zeros_like(state)
    gain_row = head_gain[:, pl.ds(pl.multiple_of(tp * DV, DV), DV)]

    @pl.loop(0, 8)
    def attend(i):
        rows = pl.ds(pl.multiple_of(i * 128, 128), 128)
        cum = lax.dot_general(
            causal, shift[rows, :], (((1,), (0,)), ((), ())),
            preferred_element_type=F32, precision=lax.Precision.HIGHEST,
        )
        v = vs[rows, :]
        k = ks[rows, :].astype(F32)
        q_dec = (qs[rows, :].astype(F32) * KEY_CHANNELS ** (-0.5) * jnp.exp(cum)).astype(BF16)
        k_dec = (k * jnp.exp(-cum)).astype(BF16)
        scores = dot(q_dec, k_dec, (((1,), (1,)), ((), ())))
        scores = jnp.where(causal > 0.5, scores, 0.0).astype(BF16)
        inner = dot(scores, v)
        s = state[...]
        carried = []
        for b in range(2):
            part = slice(b * BLK, (b + 1) * BLK)
            tot = cum[(b + 1) * BLK - 1 : (b + 1) * BLK, :]
            carried.append(dot(q_dec[part], s.astype(BF16), (((1,), (1,)), ((), ()))))
            weighted = (k[part] * jnp.exp(tot - cum[part])).astype(BF16)
            s = jnp.exp(tot) * s + dot(v[part], weighted, (((0,), (0,)), ((), ())))
        state[...] = s
        head = inner + jnp.concatenate(carried, axis=0)
        gated[rows, :] = rms_norm(head, gain_row).astype(BF16)

    second_phase(UP)
    second_phase(DOWN)
    arrived(OUT)

    def col_pair(buf, f):
        left, right = buf[f // 4, f % 4], buf[f // 4, f % 4 + 1]
        depth = left.shape[0] * left.shape[1]
        return jnp.concatenate([left.reshape(depth, 128), right.reshape(depth, 128)], axis=1)

    def partial_out(chip, x, buf, keep, send_buf):
        for f in range(0, 16, 2):
            cols = slice(f * 128, f * 128 + 256)
            part = dot(x, col_pair(buf, f)).astype(BF16)
            keep_it = jnp.where(tc == 0, part[:128], part[128:])
            give_it = jnp.where(tc == 0, part[128:], part[:128])
            keep[chip, :, cols] = keep_it
            send_buf[chip, :, cols] = give_it

    @pl.loop(0, 4)
    def mix(i):
        chip = lax.rem(ty + 2 + i, 4)
        x = gated[pl.ds(pl.multiple_of(chip * 256, 256), 256), :]
        partial_out(chip, x, wo, keep1, send1)
        push(send1.at[chip], cross1.at[chip], x1_send.at[chip], x1_recv.at[chip], other)

    @pl.loop(0, 4)
    def scatter1(i):
        chip = lax.rem(ty + jnp.where(i == 0, 2, jnp.where(i == 1, 1, jnp.where(i == 2, 3, 0))), 4)
        await_bytes(cross1.at[chip], x1_recv.at[chip])

        @pl.when(i < 3)
        def _():
            keep1[chip] = (keep1[chip].astype(F32) + cross1[chip].astype(F32)).astype(BF16)
            push(keep1.at[chip], recv1.at[ty], r1_send.at[chip], r1_recv.at[ty], {"ty": chip})

    hidden[...] = tok[...].astype(F32) + (keep1[ty].astype(F32) + cross1[ty].astype(F32))
    for k in (1, 3, 2):
        chip = lax.rem(ty + k, 4)
        await_bytes(recv1.at[chip], r1_recv.at[chip])
        hidden[...] = hidden[...] + recv1[chip].astype(F32)

    n2[ty, tc] = rms_norm(hidden[...], ffn_gain[...]).astype(BF16)
    gather_start(n2, ag2_send, ag2_recv)
    arrived(GATE)
    arrived(UP)
    arrived(DOWN)

    def finish_chunk(chip):
        await_bytes(cross2.at[chip], x2_recv.at[chip])
        keep2[chip] = (keep2[chip].astype(F32) + cross2[chip].astype(F32)).astype(BF16)
        push(keep2.at[chip], recv2.at[ty], r2_send.at[chip], r2_recv.at[ty], {"ty": chip})

    @pl.loop(0, 4)
    def feed(i):
        chip = gather_next(n2, ag2_send, ag2_recv, i)
        x = n2[chip].reshape(256, 2048)
        for lo, width in ((0, 256), (256, 256), (512, 192)):
            g = dot(x, wg[:, :, :, :, pl.ds(lo, width)].reshape(2048, width))
            u = dot(x, wu[:, :, :, :, pl.ds(lo, width)].reshape(2048, width))
            act[:, pl.ds(lo, width)] = (g * (1.0 / (1.0 + jnp.exp(-g))) * u).astype(BF16)
        partial_out(chip, act[...], wd, keep2, send2)
        push(send2.at[chip], cross2.at[chip], x2_send.at[chip], x2_recv.at[chip], other)

        @pl.when(i > 1)
        def _():
            finish_chunk(lax.rem(ty + order(i - 1), 4))

    finish_chunk(lax.rem(ty + 2, 4))
    await_bytes(cross2.at[ty], x2_recv.at[ty])
    hidden[...] = hidden[...] + (keep2[ty].astype(F32) + cross2[ty].astype(F32))
    total = hidden[...]
    for k in (1, 3, 2):
        chip = lax.rem(ty + k, 4)
        await_bytes(recv2.at[chip], r2_recv.at[chip])
        total = total + recv2[chip].astype(F32)
    out[...] = total

    for g in range(5):
        for phase, view in ((0, three), (1, three), (2, twelve), (3, twelve)):
            await_bytes(view(weights[g]), w_send.at[g, phase])
    gather_finish(n1, ag1_send)
    gather_finish(n2, ag2_send)
    for chip in range(4):
        await_bytes(send1.at[chip], x1_send.at[chip])
        await_bytes(send2.at[chip], x2_send.at[chip])
    for k in range(1, 4):
        chip = lax.rem(ty + k, 4)
        await_bytes(keep1.at[chip], r1_send.at[chip])
        await_bytes(keep2.at[chip], r2_send.at[chip])


def per_device(
    tokens, mix_gain, w_query, w_key, w_value, w_decay_down, w_decay_up, decay_bias, decay_shift,
    head_gain, w_mix_out, ffn_gain, w_gate, w_up, w_down,
):
    any_space = pl.BlockSpec(memory_space=pl.ANY)
    vmem = pl.BlockSpec(memory_space=pltpu.VMEM)
    dma = pltpu.SemaphoreType.DMA
    rows = [pltpu.VMEM((4, 128, 2048), BF16)] * 8
    return pl.pallas_call(
        kernel,
        out_shape=jax.ShapeDtypeStruct((128, 2048), F32),
        in_specs=[any_space] * 9 + [vmem] * 6,
        out_specs=vmem,
        scratch_shapes=[
            pltpu.VMEM((4, 4, 4, 32, 512), BF16),
            pltpu.VMEM((4, 4, 4, 64, 128), BF16),
            pltpu.VMEM((4, 4, 4, 32, 704), BF16),
            pltpu.VMEM((4, 4, 4, 32, 704), BF16),
            pltpu.VMEM((4, 4, 4, 176, 128), BF16),
            pltpu.VMEM((128, 2048), BF16),
            pltpu.VMEM((1024, 128), F32),
            pltpu.VMEM((4, 2, 128, 2048), BF16),
            pltpu.VMEM((4, 2, 128, 2048), BF16),
            pltpu.VMEM((1024, 128), BF16),
            pltpu.VMEM((1024, 128), BF16),
            pltpu.VMEM((1024, 256), BF16),
            pltpu.VMEM((1024, 256), BF16),
            pltpu.VMEM((256, 128), F32),
            pltpu.VMEM((128, 2048), F32),
            pltpu.VMEM((256, 704), BF16),
            *rows,
            dma((9,)), dma((5, 4)), dma((5, 4)),
            dma((7,)), dma((8,)), dma((7,)), dma((8,)),
            *([dma((4,))] * 8),
        ],
        compiler_params=pltpu.CompilerParams(
            collective_id=0, has_side_effects=True, vmem_limit_bytes=60 * 1024 * 1024
        ),
    )(
        tokens,
        decay_shift,
        w_query.reshape(4, 32, 128),
        w_key.reshape(4, 32, 128),
        w_value.reshape(4, 32, 256),
        w_mix_out.reshape(4, 64, 128),
        w_gate.reshape(4, 32, 704),
        w_up.reshape(4, 32, 704),
        w_down.reshape(4, 176, 128),
        mix_gain.reshape(1, -1),
        ffn_gain.reshape(1, -1),
        head_gain.reshape(1, -1),
        w_decay_down,
        w_decay_up,
        decay_bias.reshape(1, -1),
    )


def solution(mesh):
    finer = Mesh(mesh.devices.reshape(mesh.shape["rep"], 4, 4, 4, 2), AXES)
    everything, fs, tp = AXES, ("fz", "fx"), ("ty", "tc")
    return jax.shard_map(
        per_device,
        mesh=finer,
        in_specs=(
            P(everything, None), P(), P(fs, tp), P(fs, tp), P(fs, tp), P(), P(), P(),
            P(("rep", *fs), tp), P(), P(tp, fs), P(), P(fs, tp), P(fs, tp), P(tp, fs),
        ),
        out_specs=P(everything, None),
        check_vma=False,
    )
```

time: 377 us -> 146 us (0.39)
  the two profiles are of different devices: /device:TPU:1 before, /device:TPU:9 now
where the time goes in v1:
time: 146 us; the launch traced here: 145 us
  Pallas kernels  139 us (95%)
  local copies, waits for them, and re-layouts  5.99 us (4%)
    pallas_call x1, Pallas kernels, per_device(): pl.pallas_call(kernel, out_shape=jax.ShapeDtypeStruct((128, 2048), F32),...  139 us
    unnamed x8, local copies, waits for them, and re-layouts  5.99 us

profile of v1, /device:TPU:9, one launch (start us, length us, event | category | flops | bytes accessed | tf_op | source)
XLA Modules:
  0.0 145.3 jit_solution(12187785067776780140)
XLA Ops:
  0.0 0.0 copy-start
  0.0 1.8 %copy.16 = bf16[128,704]{1,0:T(8,128)(2,1)} copy(bf16[128,704]{0,1:T(8,128)(2,1)} %param.27) | data formatting | bytes 360448 | tf_op args[12]
  1.8 0.0 copy-done
  1.8 0.0 copy-start.1
  1.8 0.8 copy.17
  2.6 0.1 copy-done.1
  2.7 1.0 copy.18.down_proj
  3.7 139.3 %shard_map.145 = f32[128,2048]{1,0:T(8,128)} custom-call(bf16[128,2048]{1,0:T(8,128)(2,1)} %tokens_hbm.1, f32[1024,128]{1,0:T(8,128)} %shift_hbm.1, bf16[4,32,128]{2,1,0:T(8,128)(2,1)} %bitcast.16, bf16[4,32,128]{2,1,0:T(8,128)(2,1)} %bitcast.17, bf16[4,32,256]{2,1,0:T(8,128)(2,1)} %bitcast.14, bf16[4,64,128]{2,1,0:T(8,128)(2,1)} %bitcast.15, ...), custom_call_target="tpu_custom_call" | custom-call | tf_op jit(solution)/shard_map/pallas_call | solution.py:325
  143.0 2.3 %copy.20 = f32[128,2048]{1,0:T(8,128)} copy(f32[128,2048]{1,0:T(8,128)} %shard_map.145) | data formatting | bytes 2097152
Async XLA Ops:
  0.0 1.8 %copy-start = (bf16[128,704]{0,1:T(8,128)(2,1)S(1)}, bf16[128,704]{0,1:T(8,128)(2,1)}, u32[]{:S(2)}) copy-start(bf16[128,704]{0,1:T(8,128)(2,1)} %param.28) | copy-start | bytes 540676
  1.8 0.9 copy-start.1

commit v2 on v1

v2 whole, which is shorter than its diff:
```python
import jax
import jax.numpy as jnp
from jax import lax
from jax.experimental import pallas as pl
from jax.experimental.pallas import tpu as pltpu
from jax.sharding import Mesh
from jax.sharding import PartitionSpec as P

AXES = ("rep", "fz", "fx", "ty", "tc")
MESH = pl.DeviceIdType.MESH
KEY_CHANNELS = 128
DV = 256
BLK = 64
EPS = 1e-06
TAU = 16.0
F32 = jnp.float32
BF16 = jnp.bfloat16
NT = (((1,), (1,)), ((), ()))
TN = (((0,), (0,)), ((), ()))
QKV, OUT, GU0, GU1, DOWN = range(5)
QUARTERS = ((32, 512), (64, 128), (32, 768), (32, 640), (176, 128))


def rms_norm(values, gain):
    return values * lax.rsqrt(jnp.mean(values * values, axis=-1, keepdims=True) + EPS) * gain


def dot(a, b, dims=(((1,), (0,)), ((), ()))):
    return lax.dot_general(a, b, dims, preferred_element_type=F32)


def kernel(
    tokens_hbm, shift_hbm, wq_hbm, wk_hbm, wv_hbm, wo_hbm, wg_hbm, wu_hbm, wd_hbm,
    mix_gain, ffn_gain, head_gain, down_proj, up_proj, bias,
    out,
    wqkv, wo, wgu0, wgu1, wd, gate_t, up_t,
    tok, shift, n1, n2, qs, ks, vs, gated, state, hidden, act,
    part1, cross1, fold1, recv1, part2, cross2, fold2, recv2,
    loc_sem, w_send, w_recv,
    ag1_send, ag1_recv, ag2_send, ag2_recv,
    x1_send, x1_recv, r1_send, r1_recv, x2_send, x2_recv, r2_send, r2_recv,
):
    rep, fz, fx = lax.axis_index("rep"), lax.axis_index("fz"), lax.axis_index("fx")
    ty, tc = lax.axis_index("ty"), lax.axis_index("tc")
    tp = ty * 2 + tc
    weights = (wqkv, wo, wgu0, wgu1, wd)
    every = slice(None)

    def at_x(k):
        return {"fx": lax.rem(fx + k + 4, 4)}

    def at_z(k):
        whole = lax.rem(rep * 4 + fz + k + 8, 8)
        return {"rep": whole // 4, "fz": lax.rem(whole, 4)}

    def at_y(k):
        return {"ty": lax.rem(ty + k + 4, 4)}

    def chip_at(k):
        return lax.rem(ty + k + 4, 4)

    other = {"tc": 1 - tc}

    mine = [
        pltpu.make_async_copy(tokens_hbm, tok, loc_sem.at[0]),
        pltpu.make_async_copy(wq_hbm, wqkv.at[fz, fx, :, :, pl.ds(0, 128)], loc_sem.at[1]),
        pltpu.make_async_copy(wk_hbm, wqkv.at[fz, fx, :, :, pl.ds(128, 128)], loc_sem.at[2]),
        pltpu.make_async_copy(wv_hbm, wqkv.at[fz, fx, :, :, pl.ds(256, 256)], loc_sem.at[3]),
        pltpu.make_async_copy(wo_hbm, wo.at[fz, fx], loc_sem.at[4]),
        pltpu.make_async_copy(wg_hbm, gate_t, loc_sem.at[5]),
        pltpu.make_async_copy(wu_hbm, up_t, loc_sem.at[6]),
        pltpu.make_async_copy(wd_hbm, wd.at[fz, fx], loc_sem.at[7]),
        pltpu.make_async_copy(shift_hbm, shift, loc_sem.at[8]),
    ]
    for copy in mine:
        copy.start()

    barrier = pltpu.get_barrier_semaphore()
    peers = [at_x(1), at_x(2), at_x(3), at_z(1), at_z(-1), at_z(2), at_z(-2), at_y(1), at_y(3), other]
    for peer in peers:
        pl.semaphore_signal(barrier, inc=1, device_id=peer, device_id_type=MESH)

    mine[0].wait()
    normed = rms_norm(tok[...].astype(F32), mix_gain[...]).astype(BF16)
    n1[ty, tc] = normed.reshape(2, 64, 2048)
    for copy in mine[1:8]:
        copy.wait()

    pl.semaphore_wait(barrier, len(peers))

    def push(src, dst, send, recv, peer):
        pltpu.make_async_remote_copy(
            src_ref=src, dst_ref=dst, send_sem=send, recv_sem=recv, device_id=peer, device_id_type=MESH
        ).start()

    def await_bytes(view, sem):
        pltpu.make_async_copy(view, view, sem).wait()

    def spread(g, phase, z, x, first, count, peer):
        piece = weights[g].at[z, x, pl.ds(first, count)]
        push(piece, piece, w_send.at[g, phase], w_recv.at[g, phase], peer)

    def halves(g, phase):
        buf = weights[g]
        if phase < 2:
            return buf.at[0, pl.ds(0, 3), pl.ds(0, 2)]
        if phase < 4:
            return buf.at[pl.ds(0, 2), :, pl.ds(0, 2)]
        return buf.at[0, :, pl.ds(0, 2)]

    def landed(g, *phases):
        for phase in phases:
            await_bytes(halves(g, phase), w_recv.at[g, phase])

    def first_phase(g):
        for k in (1, -1, 2):
            spread(g, 0, fz, fx, 0, 2, at_x(k))
        for k in (1, -1):
            spread(g, 1, fz, fx, 2, 2, at_z(k))
        spread(g, 1, fz, fx, 2, 1, at_z(2))
        spread(g, 1, fz, fx, 3, 1, at_z(-2))

    def second_phase(g):
        landed(g, 0, 1)
        for k in (1, -1):
            spread(g, 2, fz, every, 0, 2, at_z(k))
            spread(g, 3, every, fx, 2, 2, at_x(k))

    def third_phase(g):
        landed(g, 2, 3)
        spread(g, 4, lax.rem(fz + 3, 4), every, 0, 1, at_z(1))
        spread(g, 4, lax.rem(fz + 1, 4), every, 1, 1, at_z(-1))
        spread(g, 5, every, lax.rem(fx + 3, 4), 2, 1, at_x(1))
        spread(g, 5, every, lax.rem(fx + 1, 4), 3, 1, at_x(-1))

    def complete(g):
        landed(g, 4, 5)

    class Gather:
        def __init__(self, buf, send, recv):
            self.buf, self.send, self.recv = buf, send, recv

        def some(self, j, chip, core, h, first, count, peer):
            piece = self.buf.at[chip, core, h, pl.ds(first, count)]
            push(piece, piece, self.send.at[j], self.recv.at[chip, core, h], peer)

        def half(self, j, chip, core, h, peer):
            self.some(j, chip, core, h, 0, 64, peer)

        def came(self, chip, core, h):
            await_bytes(self.buf.at[chip, core, h], self.recv.at[chip, core, h])

        def start(self):
            self.half(0, ty, tc, 0, at_y(1))
            self.half(1, ty, tc, 1, at_y(-1))
            self.half(2, ty, tc, 0, other)
            self.half(3, ty, tc, 1, other)
            self.some(4, ty, tc, 1, 0, 32, at_y(1))
            self.some(5, ty, tc, 0, 0, 32, at_y(-1))

        def step1(self):
            back, ahead = chip_at(-1), chip_at(1)
            self.came(back, tc, 0)
            self.half(6, back, tc, 0, at_y(1))
            self.some(14, ty, tc, 1, 32, 32, at_y(1))
            self.half(7, back, tc, 0, other)
            self.came(ahead, tc, 1)
            self.half(8, ahead, tc, 1, at_y(-1))
            self.some(15, ty, tc, 0, 32, 32, at_y(-1))
            self.half(9, ahead, tc, 1, other)

        def step2(self):
            far = chip_at(2)
            self.came(far, tc, 0)
            self.half(12, far, tc, 0, other)
            self.came(far, tc, 1)
            self.half(13, far, tc, 1, other)

        def step3(self):
            back, ahead = chip_at(-1), chip_at(1)
            self.came(back, tc, 1)
            self.half(10, back, tc, 1, other)
            self.came(ahead, tc, 0)
            self.half(11, ahead, tc, 0, other)

        def theirs(self, chip):
            self.came(chip, 1 - tc, 0)
            self.came(chip, 1 - tc, 1)

        def drain(self):
            for j in (0, 1, 2, 3, 6, 7, 8, 9, 10, 11, 12, 13):
                await_bytes(self.buf.at[0, 0, 0], self.send.at[j])
            for j in (4, 5, 14, 15):
                await_bytes(self.buf.at[0, 0, 0, pl.ds(0, 32)], self.send.at[j])

    class Scatter:
        def __init__(self, part, cross, fold, recv, x_send, x_recv, r_send, r_recv):
            self.part, self.cross, self.fold, self.recv = part, cross, fold, recv
            self.x_send, self.x_recv, self.r_send, self.r_recv = x_send, x_recv, r_send, r_recv

        def swap(self, chip, h):
            push(
                self.part.at[chip, 1 - tc, h], self.cross.at[chip, h],
                self.x_send.at[chip, h], self.x_recv.at[chip, h], other,
            )

        def both(self, chip, h):
            await_bytes(self.cross.at[chip, h], self.x_recv.at[chip, h])
            return self.part[chip, tc, h].astype(F32) + self.cross[chip, h].astype(F32)

        def send(self, j, chip, h, dst, k):
            push(self.part.at[chip, tc, h], dst, self.r_send.at[j], self.r_recv.at[j], at_y(k))

        def far(self):
            chip = chip_at(2)
            for h, k in ((0, 1), (1, -1)):
                self.part[chip, tc, h] = self.both(chip, h).astype(BF16)
                self.send(h, chip, h, self.fold.at[h], k)

        def near(self):
            for d, h, k in ((0, 1, 1), (1, 0, -1)):
                chip = chip_at(k)
                self.part[chip, tc, h] = self.both(chip, h).astype(BF16)
                self.send(2 + d, chip, h, self.recv.at[d, h], k)

        def ready(self):
            for h, k in ((0, 1), (1, -1)):
                chip = chip_at(k)
                self.part[chip, tc, h] = self.both(chip, h).astype(BF16)

        def through(self):
            for d, h, k in ((0, 0, 1), (1, 1, -1)):
                chip = chip_at(k)
                await_bytes(self.fold.at[d], self.r_recv.at[d])
                whole = self.part[chip, tc, h].astype(F32) + self.fold[d].astype(F32)
                self.part[chip, tc, h] = whole.astype(BF16)
                self.send(4 + d, chip, h, self.recv.at[d, h], k)

        def own(self):
            return jnp.concatenate([self.both(ty, 0), self.both(ty, 1)], axis=0)

        def total(self):
            for j in range(2, 6):
                await_bytes(self.fold.at[0], self.r_recv.at[j])
            return (self.recv[0].astype(F32) + self.recv[1].astype(F32)).reshape(128, 2048)

        def drain(self):
            for chip in range(4):
                for h in range(2):
                    await_bytes(self.cross.at[chip, h], self.x_send.at[chip, h])
            for j in range(6):
                await_bytes(self.fold.at[0], self.r_send.at[j])

    gather1 = Gather(n1, ag1_send, ag1_recv)
    gather2 = Gather(n2, ag2_send, ag2_recv)
    scatter1 = Scatter(part1, cross1, fold1, recv1, x1_send, x1_recv, r1_send, r1_recv)
    scatter2 = Scatter(part2, cross2, fold2, recv2, x2_send, x2_recv, r2_send, r2_recv)

    with jax.named_scope("start"):
        gather1.start()
        first_phase(QKV)

    with jax.named_scope("turn"):
        def turned(ref, first):
            return ref[pl.ds(first, 256), :].T.reshape(4, 32, 256)

        def mixed(first, count):
            both = jnp.concatenate([gate_t[pl.ds(first, count), :], up_t[pl.ds(first, count), :]], axis=0)
            return both.T.reshape(4, 32, 2 * count)

        wgu0[fz, fx, :, :, 0:256] = turned(gate_t, 0)
        wgu0[fz, fx, :, :, 256:512] = turned(up_t, 0)
        wgu0[fz, fx, :, :, 512:768] = mixed(512, 128)
        wgu1[fz, fx, :, :, 0:256] = turned(gate_t, 256)
        wgu1[fz, fx, :, :, 256:512] = turned(up_t, 256)
        wgu1[fz, fx, :, :, 512:640] = mixed(640, 64)

    with jax.named_scope("second_qkv"):
        second_phase(QKV)
        first_phase(OUT)
    with jax.named_scope("ag1_step1"):
        gather1.step1()
    with jax.named_scope("third_qkv"):
        third_phase(QKV)
    with jax.named_scope("second_out"):
        second_phase(OUT)
        first_phase(GU0)
        first_phase(GU1)
    with jax.named_scope("ag1_step2"):
        gather1.step2()
        mine[8].wait()
        gather1.theirs(ty)
    with jax.named_scope("complete_qkv"):
        complete(QKV)

    @pl.loop(0, 4)
    def project(i):
        chip = chip_at(jnp.where(i == 0, 0, jnp.where(i == 1, 2, jnp.where(i == 2, 1, 3))))
        with jax.named_scope("project_wait"):
            @pl.when(i == 2)
            def _():
                gather1.step3()

            @pl.when(i > 0)
            def _():
                gather1.theirs(chip)

        with jax.named_scope("project"):
            rows = pl.ds(pl.multiple_of(chip * 256, 256), 256)
            x = n1[chip].reshape(256, 2048)
            both = dot(x, wqkv[:, :, :, :, pl.ds(0, 256)].reshape(2048, 256))
            qs[rows, :] = both[:, :128].astype(BF16)
            ks[rows, :] = both[:, 128:].astype(BF16)
            vs[rows, :] = dot(x, wqkv[:, :, :, :, pl.ds(256, 256)].reshape(2048, 256)).astype(BF16)
            low = dot(x, down_proj[...], NT).astype(BF16)
            cols = pl.ds(pl.multiple_of(tp * 128, 128), 128)
            pre = dot(low, up_proj[:, cols]) + bias[:, cols]
            soft = jnp.minimum(pre, 0.0) - jnp.log1p(jnp.exp(-jnp.abs(pre)))
            shift[rows, :] = soft / TAU + shift[rows, :]

    with jax.named_scope("third_out_second_gu0"):
        third_phase(OUT)
        second_phase(GU0)

    ri = lax.broadcasted_iota(jnp.int32, (128, 128), 0)
    ci = lax.broadcasted_iota(jnp.int32, (128, 128), 1)
    causal = jnp.where((ri >= ci) & (ri // BLK == ci // BLK), 1.0, 0.0).astype(F32)
    state[...] = jnp.zeros_like(state)
    gain_row = head_gain[:, pl.ds(pl.multiple_of(tp * DV, DV), DV)]

    @pl.loop(0, 8, unroll=2)
    def attend(i):
        with jax.named_scope("attend"):
            rows = pl.ds(pl.multiple_of(i * 128, 128), 128)
            cum = lax.dot_general(
                causal, shift[rows, :], (((1,), (0,)), ((), ())),
                preferred_element_type=F32, precision=lax.Precision.HIGHEST,
            )
            v = vs[rows, :]
            k = ks[rows, :].astype(F32)
            q_dec = (qs[rows, :].astype(F32) * KEY_CHANNELS ** (-0.5) * jnp.exp(cum)).astype(BF16)
            k_dec = (k * jnp.exp(-cum)).astype(BF16)
            scores = dot(q_dec, k_dec, NT)
            scores = jnp.where(causal > 0.5, scores, 0.0).astype(BF16)
            inner = dot(scores, v)
            s = state[...]
            carried = []
            for b in range(2):
                part = slice(b * BLK, (b + 1) * BLK)
                tot = cum[(b + 1) * BLK - 1 : (b + 1) * BLK, :]
                carried.append(dot(q_dec[part], s.astype(BF16), NT))
                weighted = (k[part] * jnp.exp(tot - cum[part])).astype(BF16)
                s = jnp.exp(tot) * s + dot(v[part], weighted, TN)
            state[...] = s
            head = inner + jnp.concatenate(carried, axis=0)
            gated[rows, :] = rms_norm(head, gain_row).astype(BF16)

    with jax.named_scope("second_gu1"):
        second_phase(GU1)
        first_phase(DOWN)
    with jax.named_scope("complete_out"):
        complete(OUT)

    def partial_out(x, buf, scatter, places):
        for f in range(0, 16, 2):
            left, right = buf[f // 4, f % 4], buf[f // 4, f % 4 + 1]
            depth = left.shape[0] * left.shape[1]
            w = jnp.concatenate([left.reshape(depth, 128), right.reshape(depth, 128)], axis=1)
            product = dot(x, w).astype(BF16)
            for p, (chip, core, h) in enumerate(places):
                scatter.part[chip, core, h, :, f * 128 : f * 128 + 256] = product[p * 64 : p * 64 + 64]
        for chip, core, h in places:
            if core == 0:
                scatter.swap(chip, h)

    def whole_chip(chip):
        return [(chip, 0, 0), (chip, 0, 1), (chip, 1, 0), (chip, 1, 1)]

    def by_halves(chip):
        return [(chip, 0, 0), (chip, 1, 0), (chip, 0, 1), (chip, 1, 1)]

    def two_halves(h_back):
        back, ahead = chip_at(-1), chip_at(1)
        return [(back, 0, h_back), (back, 1, h_back), (ahead, 0, 1 - h_back), (ahead, 1, 1 - h_back)]

    @pl.loop(0, 4)
    def mix(i):
        with jax.named_scope("mix"):
            chip = chip_at(jnp.where(i == 0, 2, jnp.where(i == 1, 1, jnp.where(i == 2, 3, 0))))
            x = gated[pl.ds(pl.multiple_of(chip * 256, 256), 256), :]
            partial_out(x, wo, scatter1, whole_chip(chip))

    with jax.named_scope("rs1_far"):
        scatter1.far()
    with jax.named_scope("rs1_near"):
        scatter1.near()
        scatter1.ready()
        hidden[...] = tok[...].astype(F32) + scatter1.own()
    with jax.named_scope("third_gu0"):
        third_phase(GU0)
    with jax.named_scope("rs1_through"):
        scatter1.through()
    with jax.named_scope("third_gu1"):
        third_phase(GU1)
    with jax.named_scope("second_down"):
        second_phase(DOWN)
    with jax.named_scope("rs1_total"):
        hidden[...] = hidden[...] + scatter1.total()
    with jax.named_scope("norm2"):
        n2[ty, tc] = rms_norm(hidden[...], ffn_gain[...]).astype(BF16).reshape(2, 64, 2048)
        gather2.start()

    def gate_up(slot, x):
        def product(buf, first, width):
            return dot(x, buf[:, :, :, :, pl.ds(first, width)].reshape(2048, width))

        def gate(g, u):
            return (g * (1.0 / (1.0 + jnp.exp(-g))) * u).astype(BF16)

        act[slot, :, 0:256] = gate(product(wgu0, 0, 256), product(wgu0, 256, 256))
        act[slot, :, 256:512] = gate(product(wgu1, 0, 256), product(wgu1, 256, 256))
        both = product(wgu0, 512, 256)
        act[slot, :, 512:640] = gate(both[:, :128], both[:, 128:])
        both = product(wgu1, 512, 128)
        act[slot, :, 640:704] = gate(both, pltpu.roll(both, 64, 1))[:, :64]

    @pl.loop(0, 4)
    def feed(i):
        with jax.named_scope("feed_wait"):
            @pl.when(i == 0)
            def _():
                gather2.theirs(ty)
                gather2.step1()
                complete(GU0)
                complete(GU1)

            @pl.when(i == 1)
            def _():
                third_phase(DOWN)
                gather2.came(chip_at(-1), 1 - tc, 0)
                gather2.came(chip_at(1), 1 - tc, 1)
                gather2.step2()

            @pl.when(i == 2)
            def _():
                gather2.theirs(chip_at(2))

        with jax.named_scope("rs2_adds"):
            @pl.when(i == 3)
            def _():
                complete(DOWN)
                partial_out(act[2], wd, scatter2, by_halves(chip_at(2)))
                gather2.step3()
                partial_out(act[1], wd, scatter2, two_halves(0))
                scatter2.far()
                gather2.came(chip_at(-1), 1 - tc, 1)
                gather2.came(chip_at(1), 1 - tc, 0)

        with jax.named_scope("gate_up"):
            chip_a = chip_at(jnp.where(i == 0, 0, jnp.where(i == 2, 2, -1)))
            chip_b = chip_at(jnp.where(i == 0, 0, jnp.where(i == 2, 2, 1)))
            h_a = jnp.where(i == 3, 1, 0)
            gate_up(i, jnp.concatenate([n2[chip_a, :, h_a].reshape(128, 2048), n2[chip_b, :, 1 - h_a].reshape(128, 2048)], axis=0))

    with jax.named_scope("rs2_near"):
        scatter2.near()
    with jax.named_scope("down_b"):
        partial_out(act[3], wd, scatter2, two_halves(1))
    with jax.named_scope("down_own"):
        partial_out(act[0], wd, scatter2, by_halves(ty))
    with jax.named_scope("rs2_ready"):
        scatter2.ready()
        hidden[...] = hidden[...] + scatter2.own()
    with jax.named_scope("rs2_through"):
        scatter2.through()
    with jax.named_scope("rs2_total"):
        out[...] = hidden[...] + scatter2.total()

    with jax.named_scope("drain"):
        for g in range(5):
            for phase in range(6):
                await_bytes(halves(g, phase), w_send.at[g, phase])
        gather1.drain()
        gather2.drain()
        scatter1.drain()
        scatter2.drain()


def per_device(
    tokens, mix_gain, w_query, w_key, w_value, w_decay_down, w_decay_up, decay_bias, decay_shift,
    head_gain, w_mix_out, ffn_gain, w_gate, w_up, w_down,
):
    any_space = pl.BlockSpec(memory_space=pl.ANY)
    vmem = pl.BlockSpec(memory_space=pltpu.VMEM)
    dma = pltpu.SemaphoreType.DMA
    scatter = [
        pltpu.VMEM((4, 2, 2, 64, 2048), BF16),
        pltpu.VMEM((4, 2, 64, 2048), BF16),
        pltpu.VMEM((2, 64, 2048), BF16),
        pltpu.VMEM((2, 2, 64, 2048), BF16),
    ]
    return pl.pallas_call(
        kernel,
        out_shape=jax.ShapeDtypeStruct((128, 2048), F32),
        in_specs=[any_space] * 9 + [vmem] * 6,
        out_specs=vmem,
        scratch_shapes=[
            *[pltpu.VMEM((4, 4, 4, *quarter), BF16) for quarter in QUARTERS],
            pltpu.VMEM((704, 128), BF16),
            pltpu.VMEM((704, 128), BF16),
            pltpu.VMEM((128, 2048), BF16),
            pltpu.VMEM((1024, 128), F32),
            pltpu.VMEM((4, 2, 2, 64, 2048), BF16),
            pltpu.VMEM((4, 2, 2, 64, 2048), BF16),
            pltpu.VMEM((1024, 128), BF16),
            pltpu.VMEM((1024, 128), BF16),
            pltpu.VMEM((1024, 256), BF16),
            pltpu.VMEM((1024, 256), BF16),
            pltpu.VMEM((256, 128), F32),
            pltpu.VMEM((128, 2048), F32),
            pltpu.VMEM((4, 256, 704), BF16),
            *scatter, *scatter,
            dma((9,)), dma((5, 6)), dma((5, 6)),
            dma((16,)), dma((4, 2, 2)), dma((16,)), dma((4, 2, 2)),
            dma((4, 2)), dma((4, 2)), dma((6,)), dma((6,)),
            dma((4, 2)), dma((4, 2)), dma((6,)), dma((6,)),
        ],
        compiler_params=pltpu.CompilerParams(
            collective_id=0, has_side_effects=True, vmem_limit_bytes=60 * 1024 * 1024
        ),
    )(
        tokens,
        decay_shift,
        w_query.reshape(4, 32, 128),
        w_key.reshape(4, 32, 128),
        w_value.reshape(4, 32, 256),
        w_mix_out.reshape(4, 64, 128),
        w_gate.T,
        w_up.T,
        w_down.reshape(4, 176, 128),
        mix_gain.reshape(1, -1),
        ffn_gain.reshape(1, -1),
        head_gain.reshape(1, -1),
        w_decay_down.T,
        w_decay_up,
        decay_bias.reshape(1, -1),
    )


def solution(mesh):
    finer = Mesh(mesh.devices.reshape(mesh.shape["rep"], 4, 4, 4, 2), AXES)
    everything, fs, tp = AXES, ("fz", "fx"), ("ty", "tc")
    return jax.shard_map(
        per_device,
        mesh=finer,
        in_specs=(
            P(everything, None), P(), P(fs, tp), P(fs, tp), P(fs, tp), P(), P(), P(),
            P(("rep", *fs), tp), P(), P(tp, fs), P(), P(fs, tp), P(fs, tp), P(tp, fs),
        ),
        out_specs=P(everything, None),
        check_vma=False,
    )
```

time: 146 us -> 111 us (0.76)
  the two profiles are of different devices: /device:TPU:9 before, /device:TPU:1 now
where the time goes in v2:
time: 111 us
  Pallas kernels  109 us (98%)
  local copies, waits for them, and re-layouts  2.3 us (2%)
    pallas_call x1, Pallas kernels, per_device(): pl.pallas_call(kernel, out_shape=jax.ShapeDtypeStruct((128, 2048), F32),...  109 us
    unnamed x1, local copies, waits for them, and re-layouts  2.3 us

profile of v2, /device:TPU:1, one launch (start us, length us, event | category | flops | bytes accessed | tf_op | source)
XLA Modules:
  0.0 111.1 jit_solution(17171053429158047644)
XLA Ops:
  0.0 108.8 %shard_map.145 = f32[128,2048]{1,0:T(8,128)} custom-call(bf16[128,2048]{1,0:T(8,128)(2,1)} %tokens_hbm.1, f32[1024,128]{1,0:T(8,128)} %shift_hbm.1, bf16[4,32,128]{2,1,0:T(8,128)(2,1)} %bitcast.18, bf16[4,32,128]{2,1,0:T(8,128)(2,1)} %bitcast.19, bf16[4,32,256]{2,1,0:T(8,128)(2,1)} %bitcast.16, bf16[4,64,128]{2,1,0:T(8,128)(2,1)} %bitcast.17, ...), custom_call_target="tpu_custom_call" | custom-call | tf_op jit(solution)/shard_map/pallas_call | solution.py:502
  108.8 2.3 %copy.17 = f32[128,2048]{1,0:T(8,128)} copy(f32[128,2048]{1,0:T(8,128)} %shard_map.145) | data formatting | bytes 2097152

commit v3 on v2

--- a/solution.py
+++ b/solution.py
@@ -34,7 +34,7 @@
     mix_gain, ffn_gain, head_gain, down_proj, up_proj, bias,
     out,
     wqkv, wo, wgu0, wgu1, wd, gate_t, up_t,
-    tok, shift, n1, n2, qs, ks, vs, gated, state, hidden, act,
+    tok, shift, cums, n1, n2, qs, ks, vs, gated, state, hidden, act,
     part1, cross1, fold1, recv1, part2, cross2, fold2, recv2,
     loc_sem, w_send, w_recv,
     ag1_send, ag1_recv, ag2_send, ag2_recv,
@@ -150,24 +150,26 @@
         def came(self, chip, core, h):
             await_bytes(self.buf.at[chip, core, h], self.recv.at[chip, core, h])
 
-        def start(self):
-            self.half(0, ty, tc, 0, at_y(1))
-            self.half(1, ty, tc, 1, at_y(-1))
-            self.half(2, ty, tc, 0, other)
-            self.half(3, ty, tc, 1, other)
-            self.some(4, ty, tc, 1, 0, 32, at_y(1))
-            self.some(5, ty, tc, 0, 0, 32, at_y(-1))
+        def start(self, q):
+            rows = pl.ds(q * 32, 32)
+            own, ahead, back = self.buf.at[ty, tc], at_y(1), at_y(-1)
+            plan = [(0, ahead), (1, back), (0, other), (1, other)]
+            for j, (h, peer) in enumerate(plan):
+                push(own.at[h, rows], own.at[h, rows], self.send.at[q * 4 + j], self.recv.at[ty, tc, h], peer)
+            if q == 1:
+                self.some(14, ty, tc, 1, 0, 32, ahead)
+                self.some(15, ty, tc, 0, 0, 32, back)
 
         def step1(self):
             back, ahead = chip_at(-1), chip_at(1)
             self.came(back, tc, 0)
-            self.half(6, back, tc, 0, at_y(1))
-            self.some(14, ty, tc, 1, 32, 32, at_y(1))
-            self.half(7, back, tc, 0, other)
+            self.half(8, back, tc, 0, at_y(1))
+            self.some(16, ty, tc, 1, 32, 32, at_y(1))
+            self.half(9, back, tc, 0, other)
             self.came(ahead, tc, 1)
-            self.half(8, ahead, tc, 1, at_y(-1))
-            self.some(15, ty, tc, 0, 32, 32, at_y(-1))
-            self.half(9, ahead, tc, 1, other)
+            self.half(18, ahead, tc, 1, at_y(-1))
+            self.some(17, ty, tc, 0, 32, 32, at_y(-1))
+            self.half(19, ahead, tc, 1, other)
 
         def step2(self):
             far = chip_at(2)
@@ -188,10 +190,9 @@
             self.came(chip, 1 - tc, 1)
 
         def drain(self):
-            for j in (0, 1, 2, 3, 6, 7, 8, 9, 10, 11, 12, 13):
-                await_bytes(self.buf.at[0, 0, 0], self.send.at[j])
-            for j in (4, 5, 14, 15):
-                await_bytes(self.buf.at[0, 0, 0, pl.ds(0, 32)], self.send.at[j])
+            for j in range(20):
+                whole = j in (8, 9, 10, 11, 12, 13, 18, 19)
+                await_bytes(self.buf.at[0, 0, 0, pl.ds(0, 64 if whole else 32)], self.send.at[j])
 
     class Scatter:
         def __init__(self, part, cross, fold, recv, x_send, x_recv, r_send, r_recv):
@@ -208,20 +209,23 @@
             await_bytes(self.cross.at[chip, h], self.x_recv.at[chip, h])
             return self.part[chip, tc, h].astype(F32) + self.cross[chip, h].astype(F32)
 
-        def send(self, j, chip, h, dst, k):
-            push(self.part.at[chip, tc, h], dst, self.r_send.at[j], self.r_recv.at[j], at_y(k))
+        def send(self, j, src, dst, k):
+            push(src, dst, self.r_send.at[j], self.r_recv.at[j], at_y(k))
 
         def far(self):
             chip = chip_at(2)
-            for h, k in ((0, 1), (1, -1)):
+            for h in range(2):
                 self.part[chip, tc, h] = self.both(chip, h).astype(BF16)
-                self.send(h, chip, h, self.fold.at[h], k)
+            for q in range(2):
+                rows = pl.ds(q * 32, 32)
+                for h, k in ((0, 1), (1, -1)):
+                    self.send(q * 2 + h, self.part.at[chip, tc, h, rows], self.fold.at[h, rows], k)
 
         def near(self):
             for d, h, k in ((0, 1, 1), (1, 0, -1)):
                 chip = chip_at(k)
                 self.part[chip, tc, h] = self.both(chip, h).astype(BF16)
-                self.send(2 + d, chip, h, self.recv.at[d, h], k)
+                self.send(4 + d, self.part.at[chip, tc, h], self.recv.at[d, h], k)
 
         def ready(self):
             for h, k in ((0, 1), (1, -1)):
@@ -229,27 +233,32 @@
                 self.part[chip, tc, h] = self.both(chip, h).astype(BF16)
 
         def through(self):
-            for d, h, k in ((0, 0, 1), (1, 1, -1)):
-                chip = chip_at(k)
-                await_bytes(self.fold.at[d], self.r_recv.at[d])
-                whole = self.part[chip, tc, h].astype(F32) + self.fold[d].astype(F32)
-                self.part[chip, tc, h] = whole.astype(BF16)
-                self.send(4 + d, chip, h, self.recv.at[d, h], k)
-
-        def own(self):
-            return jnp.concatenate([self.both(ty, 0), self.both(ty, 1)], axis=0)
-
-        def total(self):
-            for j in range(2, 6):
-                await_bytes(self.fold.at[0], self.r_recv.at[j])
-            return (self.recv[0].astype(F32) + self.recv[1].astype(F32)).reshape(128, 2048)
+            for q in range(2):
+                rows = pl.ds(q * 32, 32)
+                for d, k in ((0, 1), (1, -1)):
+                    chip = chip_at(k)
+                    await_bytes(self.fold.at[d, rows], self.r_recv.at[q * 2 + d])
+                    whole = self.part[chip, tc, d, rows].astype(F32) + self.fold[d, rows].astype(F32)
+                    self.part[chip, tc, d, rows] = whole.astype(BF16)
+                    self.send(6 + q * 2 + d, self.part.at[chip, tc, d, rows], self.recv.at[d, d, rows], k)
+
+        def total(self, q):
+            rows = pl.ds(q * 32, 32)
+            for d in range(2):
+                if q == 0:
+                    await_bytes(self.recv.at[d, 1 - d], self.r_recv.at[4 + d])
+                await_bytes(self.recv.at[d, d, rows], self.r_recv.at[6 + q * 2 + d])
+            return self.recv[0, :, rows].astype(F32) + self.recv[1, :, rows].astype(F32)
+
+        def own(self, h):
+            return self.both(ty, h)
 
         def drain(self):
             for chip in range(4):
                 for h in range(2):
                     await_bytes(self.cross.at[chip, h], self.x_send.at[chip, h])
-            for j in range(6):
-                await_bytes(self.fold.at[0], self.r_send.at[j])
+            for j in range(10):
+                await_bytes(self.fold.at[0, pl.ds(0, 64 if j in (4, 5) else 32)], self.r_send.at[j])
 
     gather1 = Gather(n1, ag1_send, ag1_recv)
     gather2 = Gather(n2, ag2_send, ag2_recv)
@@ -257,8 +266,10 @@
     scatter2 = Scatter(part2, cross2, fold2, recv2, x2_send, x2_recv, r2_send, r2_recv)
 
     with jax.named_scope("start"):
-        gather1.start()
+        gather1.start(0)
+        gather1.start(1)
         first_phase(QKV)
+        first_phase(OUT)
 
     with jax.named_scope("turn"):
         def turned(ref, first):
@@ -275,89 +286,132 @@
         wgu1[fz, fx, :, :, 256:512] = turned(up_t, 256)
         wgu1[fz, fx, :, :, 512:640] = mixed(640, 64)
 
+    def row_set(i):
+        chip_a = chip_at(jnp.where(i == 0, 0, jnp.where(i == 2, 2, -1)))
+        chip_b = chip_at(jnp.where(i == 0, 0, jnp.where(i == 2, 2, 1)))
+        h_a = jnp.where(i == 3, 1, 0)
+        return [(chip_a, 0, h_a), (chip_a, 1, h_a), (chip_b, 0, 1 - h_a), (chip_b, 1, 1 - h_a)]
+
+    def rows_of(buf, places):
+        return jnp.concatenate([buf[place] for place in places], axis=0)
+
+    def from_other(gather, places):
+        for chip, _, h in places[::2]:
+            gather.came(chip, 1 - tc, h)
+
+    def block(place):
+        chip, core, h = place
+        return chip * 4 + core * 2 + h
+
+    cols = pl.ds(pl.multiple_of(tp * 128, 128), 128)
+
+    def causal_mask(size, dtype):
+        ri = lax.broadcasted_iota(jnp.int32, (size, size), 0)
+        ci = lax.broadcasted_iota(jnp.int32, (size, size), 1)
+        return jnp.where((ri >= ci) & (ri // BLK == ci // BLK), 1.0, 0.0).astype(dtype)
+
+    def decay(places):
+        x = rows_of(n1, places)
+        low = dot(x, down_proj[...], NT).astype(BF16)
+        pre = dot(low, up_proj[:, cols]) + bias[:, cols]
+        soft = jnp.minimum(pre, 0.0) - jnp.log1p(jnp.exp(-jnp.abs(pre)))
+        logs = soft / TAU + jnp.concatenate([shift[block(place)] for place in places], axis=0)
+        one = logs.astype(BF16)
+        rest = logs - one.astype(F32)
+        two = rest.astype(BF16)
+        three = (rest - two.astype(F32)).astype(BF16)
+        sums = dot(causal_mask(256, BF16), jnp.concatenate([one, two, three], axis=1))
+        cum = sums[:, :128] + sums[:, 128:256] + sums[:, 256:]
+        for p, place in enumerate(places):
+            cums[block(place)] = cum[p * 64 : p * 64 + 64]
+
     with jax.named_scope("second_qkv"):
         second_phase(QKV)
-        first_phase(OUT)
+    with jax.named_scope("decay0"):
+        mine[8].wait()
+        own_set, first_set = row_set(0), row_set(1)
+        from_other(gather1, own_set)
+        decay(own_set)
     with jax.named_scope("ag1_step1"):
         gather1.step1()
+    with jax.named_scope("second_out"):
+        second_phase(OUT)
     with jax.named_scope("third_qkv"):
         third_phase(QKV)
-    with jax.named_scope("second_out"):
-        second_phase(OUT)
         first_phase(GU0)
-        first_phase(GU1)
+    with jax.named_scope("decay1"):
+        from_other(gather1, first_set)
+        decay(first_set)
     with jax.named_scope("ag1_step2"):
         gather1.step2()
-        mine[8].wait()
-        gather1.theirs(ty)
+    with jax.named_scope("third_out"):
+        third_phase(OUT)
+        first_phase(GU1)
     with jax.named_scope("complete_qkv"):
         complete(QKV)
 
     @pl.loop(0, 4)
     def project(i):
-        chip = chip_at(jnp.where(i == 0, 0, jnp.where(i == 1, 2, jnp.where(i == 2, 1, 3))))
+        places = row_set(i)
         with jax.named_scope("project_wait"):
             @pl.when(i == 2)
             def _():
                 gather1.step3()
 
-            @pl.when(i > 0)
+        with jax.named_scope("decay"):
+            @pl.when(i > 1)
             def _():
-                gather1.theirs(chip)
+                from_other(gather1, places)
+                decay(places)
 
         with jax.named_scope("project"):
-            rows = pl.ds(pl.multiple_of(chip * 256, 256), 256)
-            x = n1[chip].reshape(256, 2048)
-            both = dot(x, wqkv[:, :, :, :, pl.ds(0, 256)].reshape(2048, 256))
-            qs[rows, :] = both[:, :128].astype(BF16)
-            ks[rows, :] = both[:, 128:].astype(BF16)
-            vs[rows, :] = dot(x, wqkv[:, :, :, :, pl.ds(256, 256)].reshape(2048, 256)).astype(BF16)
-            low = dot(x, down_proj[...], NT).astype(BF16)
-            cols = pl.ds(pl.multiple_of(tp * 128, 128), 128)
-            pre = dot(low, up_proj[:, cols]) + bias[:, cols]
-            soft = jnp.minimum(pre, 0.0) - jnp.log1p(jnp.exp(-jnp.abs(pre)))
-            shift[rows, :] = soft / TAU + shift[rows, :]
-
-    with jax.named_scope("third_out_second_gu0"):
-        third_phase(OUT)
+            x = rows_of(n1, places)
+            both = dot(x, wqkv[:, :, :, :, pl.ds(0, 256)].reshape(2048, 256)).astype(BF16)
+            values = dot(x, wqkv[:, :, :, :, pl.ds(256, 256)].reshape(2048, 256)).astype(BF16)
+            for p, place in enumerate(places):
+                piece = slice(p * 64, p * 64 + 64)
+                qs[block(place)] = both[piece, :128]
+                ks[block(place)] = both[piece, 128:]
+                vs[block(place)] = values[piece]
+
+    with jax.named_scope("second_gu0"):
         second_phase(GU0)
-
-    ri = lax.broadcasted_iota(jnp.int32, (128, 128), 0)
-    ci = lax.broadcasted_iota(jnp.int32, (128, 128), 1)
-    causal = jnp.where((ri >= ci) & (ri // BLK == ci // BLK), 1.0, 0.0).astype(F32)
+        first_phase(DOWN)
+
+    causal = causal_mask(128, F32)
     state[...] = jnp.zeros_like(state)
     gain_row = head_gain[:, pl.ds(pl.multiple_of(tp * DV, DV), DV)]
 
-    @pl.loop(0, 8, unroll=2)
     def attend(i):
-        with jax.named_scope("attend"):
-            rows = pl.ds(pl.multiple_of(i * 128, 128), 128)
-            cum = lax.dot_general(
-                causal, shift[rows, :], (((1,), (0,)), ((), ())),
-                preferred_element_type=F32, precision=lax.Precision.HIGHEST,
-            )
-            v = vs[rows, :]
-            k = ks[rows, :].astype(F32)
-            q_dec = (qs[rows, :].astype(F32) * KEY_CHANNELS ** (-0.5) * jnp.exp(cum)).astype(BF16)
-            k_dec = (k * jnp.exp(-cum)).astype(BF16)
-            scores = dot(q_dec, k_dec, NT)
-            scores = jnp.where(causal > 0.5, scores, 0.0).astype(BF16)
-            inner = dot(scores, v)
-            s = state[...]
-            carried = []
-            for b in range(2):
-                part = slice(b * BLK, (b + 1) * BLK)
-                tot = cum[(b + 1) * BLK - 1 : (b + 1) * BLK, :]
-                carried.append(dot(q_dec[part], s.astype(BF16), NT))
-                weighted = (k[part] * jnp.exp(tot - cum[part])).astype(BF16)
-                s = jnp.exp(tot) * s + dot(v[part], weighted, TN)
-            state[...] = s
-            head = inner + jnp.concatenate(carried, axis=0)
-            gated[rows, :] = rms_norm(head, gain_row).astype(BF16)
-
-    with jax.named_scope("second_gu1"):
-        second_phase(GU1)
-        first_phase(DOWN)
+        pair = pl.ds(i * 2, 2)
+        cum = cums[pair].reshape(128, 128)
+        v = vs[pair].reshape(128, DV)
+        k = ks[pair].reshape(128, 128).astype(F32)
+        q_full = qs[pair].reshape(128, 128).astype(F32) * KEY_CHANNELS ** (-0.5) * jnp.exp(cum)
+        k_full = k * jnp.exp(-cum)
+        q_dec, k_dec = q_full.astype(BF16), k_full.astype(BF16)
+        q_low = (q_full - q_dec.astype(F32)).astype(BF16)
+        k_low = (k_full - k_dec.astype(F32)).astype(BF16)
+        scores = dot(
+            jnp.concatenate([q_dec, q_dec, q_low], axis=1),
+            jnp.concatenate([k_dec, k_low, k_dec], axis=1), NT,
+        )
+        scores = jnp.where(causal > 0.5, scores, 0.0).astype(BF16)
+        inner = dot(scores, v)
+        s = state[...]
+        carried = []
+        for b in range(2):
+            part = slice(b * BLK, (b + 1) * BLK)
+            tot = cum[(b + 1) * BLK - 1 : (b + 1) * BLK, :]
+            carried.append(dot(q_dec[part], s.astype(BF16), NT))
+            weighted = (k[part] * jnp.exp(tot - cum[part])).astype(BF16)
+            s = jnp.exp(tot) * s + dot(v[part], weighted, TN)
+        state[...] = s
+        head = inner + jnp.concatenate(carried, axis=0)
+        gated[pair] = rms_norm(head, gain_row).astype(BF16).reshape(2, BLK, DV)
+
+    with jax.named_scope("attend"):
+        pl.loop(0, 8, unroll=2)(attend)
     with jax.named_scope("complete_out"):
         complete(OUT)
 
@@ -373,42 +427,37 @@
             if core == 0:
                 scatter.swap(chip, h)
 
-    def whole_chip(chip):
-        return [(chip, 0, 0), (chip, 0, 1), (chip, 1, 0), (chip, 1, 1)]
-
-    def by_halves(chip):
-        return [(chip, 0, 0), (chip, 1, 0), (chip, 0, 1), (chip, 1, 1)]
-
-    def two_halves(h_back):
-        back, ahead = chip_at(-1), chip_at(1)
-        return [(back, 0, h_back), (back, 1, h_back), (ahead, 0, 1 - h_back), (ahead, 1, 1 - h_back)]
-
     @pl.loop(0, 4)
     def mix(i):
         with jax.named_scope("mix"):
             chip = chip_at(jnp.where(i == 0, 2, jnp.where(i == 1, 1, jnp.where(i == 2, 3, 0))))
-            x = gated[pl.ds(pl.multiple_of(chip * 256, 256), 256), :]
-            partial_out(x, wo, scatter1, whole_chip(chip))
+            x = gated[pl.ds(chip * 4, 4)].reshape(256, DV)
+            partial_out(x, wo, scatter1, [(chip, 0, 0), (chip, 0, 1), (chip, 1, 0), (chip, 1, 1)])
 
     with jax.named_scope("rs1_far"):
         scatter1.far()
     with jax.named_scope("rs1_near"):
         scatter1.near()
         scatter1.ready()
-        hidden[...] = tok[...].astype(F32) + scatter1.own()
+        for h in range(2):
+            own = tok[pl.ds(h * 64, 64), :].astype(F32) + scatter1.own(h)
+            hidden[h] = own
+    with jax.named_scope("second_gu1"):
+        second_phase(GU1)
+    with jax.named_scope("rs1_through"):
+        scatter1.through()
     with jax.named_scope("third_gu0"):
         third_phase(GU0)
-    with jax.named_scope("rs1_through"):
-        scatter1.through()
+    for q in range(2):
+        with jax.named_scope("rs1_total"):
+            rows = pl.ds(q * 32, 32)
+            values = hidden[:, rows] + scatter1.total(q)
+            hidden[:, rows] = values
+            n2[ty, tc, :, rows] = rms_norm(values, ffn_gain[...]).astype(BF16)
+            gather2.start(q)
     with jax.named_scope("third_gu1"):
         third_phase(GU1)
-    with jax.named_scope("second_down"):
         second_phase(DOWN)
-    with jax.named_scope("rs1_total"):
-        hidden[...] = hidden[...] + scatter1.total()
-    with jax.named_scope("norm2"):
-        n2[ty, tc] = rms_norm(hidden[...], ffn_gain[...]).astype(BF16).reshape(2, 64, 2048)
-        gather2.start()
 
     def gate_up(slot, x):
         def product(buf, first, width):
@@ -426,55 +475,52 @@
 
     @pl.loop(0, 4)
     def feed(i):
+        places = row_set(i)
         with jax.named_scope("feed_wait"):
             @pl.when(i == 0)
             def _():
-                gather2.theirs(ty)
                 gather2.step1()
                 complete(GU0)
                 complete(GU1)
 
-            @pl.when(i == 1)
+            @pl.when(i == 2)
             def _():
                 third_phase(DOWN)
-                gather2.came(chip_at(-1), 1 - tc, 0)
-                gather2.came(chip_at(1), 1 - tc, 1)
                 gather2.step2()
 
-            @pl.when(i == 2)
-            def _():
-                gather2.theirs(chip_at(2))
-
-        with jax.named_scope("rs2_adds"):
+        with jax.named_scope("feed_down"):
             @pl.when(i == 3)
             def _():
+                gather2.step3()
                 complete(DOWN)
-                partial_out(act[2], wd, scatter2, by_halves(chip_at(2)))
-                gather2.step3()
-                partial_out(act[1], wd, scatter2, two_halves(0))
-                scatter2.far()
-                gather2.came(chip_at(-1), 1 - tc, 1)
-                gather2.came(chip_at(1), 1 - tc, 0)
+                partial_out(act[1], wd, scatter2, row_set(1))
+                partial_out(act[2], wd, scatter2, row_set(2))
+                scatter2.near()
+
+        with jax.named_scope("feed_from"):
+            from_other(gather2, places)
 
         with jax.named_scope("gate_up"):
-            chip_a = chip_at(jnp.where(i == 0, 0, jnp.where(i == 2, 2, -1)))
-            chip_b = chip_at(jnp.where(i == 0, 0, jnp.where(i == 2, 2, 1)))
-            h_a = jnp.where(i == 3, 1, 0)
-            gate_up(i, jnp.concatenate([n2[chip_a, :, h_a].reshape(128, 2048), n2[chip_b, :, 1 - h_a].reshape(128, 2048)], axis=0))
-
-    with jax.named_scope("rs2_near"):
-        scatter2.near()
-    with jax.named_scope("down_b"):
-        partial_out(act[3], wd, scatter2, two_halves(1))
+            gate_up(i, rows_of(n2, places))
+
+    with jax.named_scope("rs2_far"):
+        scatter2.far()
+    with jax.named_scope("down_last"):
+        partial_out(act[3], wd, scatter2, row_set(3))
     with jax.named_scope("down_own"):
-        partial_out(act[0], wd, scatter2, by_halves(ty))
+        partial_out(act[0], wd, scatter2, row_set(0))
     with jax.named_scope("rs2_ready"):
         scatter2.ready()
-        hidden[...] = hidden[...] + scatter2.own()
     with jax.named_scope("rs2_through"):
         scatter2.through()
     with jax.named_scope("rs2_total"):
-        out[...] = hidden[...] + scatter2.total()
+        for h in range(2):
+            hidden[h] = hidden[h] + scatter2.own(h)
+        for q in range(2):
+            rows = pl.ds(q * 32, 32)
+            values = hidden[:, rows] + scatter2.total(q)
+            for h in range(2):
+                out[pl.ds(h * 64 + q * 32, 32), :] = values[h]
 
     with jax.named_scope("drain"):
         for g in range(5):
@@ -490,7 +536,7 @@
     tokens, mix_gain, w_query, w_key, w_value, w_decay_down, w_decay_up, decay_bias, decay_shift,
     head_gain, w_mix_out, ffn_gain, w_gate, w_up, w_down,
 ):
-    any_space = pl.BlockSpec(memory_space=pl.ANY)
+    hbm = pl.BlockSpec(memory_space=pltpu.HBM)
     vmem = pl.BlockSpec(memory_space=pltpu.VMEM)
     dma = pltpu.SemaphoreType.DMA
     scatter = [
@@ -501,36 +547,37 @@
     ]
     return pl.pallas_call(
         kernel,
-        out_shape=jax.ShapeDtypeStruct((128, 2048), F32),
-        in_specs=[any_space] * 9 + [vmem] * 6,
+        out_shape=pltpu.VMEM((128, 2048), F32),
+        in_specs=[hbm] * 9 + [vmem] * 6,
         out_specs=vmem,
         scratch_shapes=[
             *[pltpu.VMEM((4, 4, 4, *quarter), BF16) for quarter in QUARTERS],
             pltpu.VMEM((704, 128), BF16),
             pltpu.VMEM((704, 128), BF16),
             pltpu.VMEM((128, 2048), BF16),
-            pltpu.VMEM((1024, 128), F32),
+            pltpu.VMEM((16, BLK, 128), F32),
+            pltpu.VMEM((16, BLK, 128), F32),
             pltpu.VMEM((4, 2, 2, 64, 2048), BF16),
             pltpu.VMEM((4, 2, 2, 64, 2048), BF16),
-            pltpu.VMEM((1024, 128), BF16),
-            pltpu.VMEM((1024, 128), BF16),
-            pltpu.VMEM((1024, 256), BF16),
-            pltpu.VMEM((1024, 256), BF16),
+            pltpu.VMEM((16, BLK, 128), BF16),
+            pltpu.VMEM((16, BLK, 128), BF16),
+            pltpu.VMEM((16, BLK, DV), BF16),
+            pltpu.VMEM((16, BLK, DV), BF16),
             pltpu.VMEM((256, 128), F32),
-            pltpu.VMEM((128, 2048), F32),
+            pltpu.VMEM((2, 64, 2048), F32),
             pltpu.VMEM((4, 256, 704), BF16),
             *scatter, *scatter,
             dma((9,)), dma((5, 6)), dma((5, 6)),
-            dma((16,)), dma((4, 2, 2)), dma((16,)), dma((4, 2, 2)),
-            dma((4, 2)), dma((4, 2)), dma((6,)), dma((6,)),
-            dma((4, 2)), dma((4, 2)), dma((6,)), dma((6,)),
+            dma((20,)), dma((4, 2, 2)), dma((20,)), dma((4, 2, 2)),
+            dma((4, 2)), dma((4, 2)), dma((10,)), dma((10,)),
+            dma((4, 2)), dma((4, 2)), dma((10,)), dma((10,)),
         ],
         compiler_params=pltpu.CompilerParams(
-            collective_id=0, has_side_effects=True, vmem_limit_bytes=60 * 1024 * 1024
+            collective_id=0, has_side_effects=True, vmem_limit_bytes=58 * 1024 * 1024
         ),
     )(
         tokens,
-        decay_shift,
+        decay_shift.reshape(16, BLK, 128),
         w_query.reshape(4, 32, 128),
         w_key.reshape(4, 32, 128),
         w_value.reshape(4, 32, 256),

time: 111 us -> 106 us (0.955)
  Pallas kernels: 109 us -> 104 us
  local copies, waits for them, and re-layouts: 2.3 us -> 0.97 us
    pallas_call x1, Pallas kernels: 109 us -> 104 us  [per_device(): pl.pallas_call(kernel, out_shape=pltpu.VMEM((128, 2048), F32), in_specs=[...]
    unnamed x1, local copies, waits for them, and re-layouts: 2.3 us -> 0.97 us
where the time goes in v3:
time: 106 us; the launch traced here: 105 us
  Pallas kernels  104 us (98%)
    pallas_call x1, Pallas kernels, per_device(): pl.pallas_call(kernel, out_shape=pltpu.VMEM((128, 2048), F32), in_specs=[...  104 us

profile of v3, /device:TPU:1, one launch (start us, length us, event | category | flops | bytes accessed | tf_op | source)
XLA Modules:
  0.0 105.4 jit_solution(18220742441260589818)
XLA Ops:
  0.0 104.5 %shard_map.145 = f32[128,2048]{1,0:T(8,128)S(1)} custom-call(bf16[128,2048]{1,0:T(8,128)(2,1)} %tokens_hbm.1, f32[16,64,128]{2,1,0:T(8,128)} %bitcast.13, bf16[4,32,128]{2,1,0:T(8,128)(2,1)} %bitcast.20, bf16[4,32,128]{2,1,0:T(8,128)(2,1)} %bitcast.21, bf16[4,32,256]{2,1,0:T(8,128)(2,1)} %bitcast.18, bf16[4,64,128]{2,1,0:T(8,128)(2,1)} %bitcast.19, ...), custom_call_target="tpu_custom_call" | custom-call | tf_op jit(solution)/shard_map/pallas_call | solution.py:548
  104.5 1.0 copy.17

commit v4 on v3

--- a/solution.py
+++ b/solution.py
@@ -448,6 +448,9 @@
         scatter1.through()
     with jax.named_scope("third_gu0"):
         third_phase(GU0)
+    with jax.named_scope("third_gu1"):
+        third_phase(GU1)
+        second_phase(DOWN)
     for q in range(2):
         with jax.named_scope("rs1_total"):
             rows = pl.ds(q * 32, 32)
@@ -455,9 +458,6 @@
             hidden[:, rows] = values
             n2[ty, tc, :, rows] = rms_norm(values, ffn_gain[...]).astype(BF16)
             gather2.start(q)
-    with jax.named_scope("third_gu1"):
-        third_phase(GU1)
-        second_phase(DOWN)
 
     def gate_up(slot, x):
         def product(buf, first, width):

time: 106 us -> 106 us (level)
  no operation moved by 1% of the time
where the time goes in v4:
time: 106 us
  Pallas kernels  105 us (99%)
    pallas_call x1, Pallas kernels, per_device(): pl.pallas_call(kernel, out_shape=pltpu.VMEM((128, 2048), F32), in_specs=[...  105 us

profile of v4, /device:TPU:1, one launch (start us, length us, event | category | flops | bytes accessed | tf_op | source)
XLA Modules:
  0.0 105.5 jit_solution(3192787921314367057)
XLA Ops:
  0.0 104.6 %shard_map.145 = f32[128,2048]{1,0:T(8,128)S(1)} custom-call(bf16[128,2048]{1,0:T(8,128)(2,1)} %tokens_hbm.1, f32[16,64,128]{2,1,0:T(8,128)} %bitcast.13, bf16[4,32,128]{2,1,0:T(8,128)(2,1)} %bitcast.20, bf16[4,32,128]{2,1,0:T(8,128)(2,1)} %bitcast.21, bf16[4,32,256]{2,1,0:T(8,128)(2,1)} %bitcast.18, bf16[4,64,128]{2,1,0:T(8,128)(2,1)} %bitcast.19, ...), custom_call_target="tpu_custom_call" | custom-call | tf_op jit(solution)/shard_map/pallas_call | solution.py:548
  104.6 1.0 copy.17

commit v5 on v4

--- a/solution.py
+++ b/solution.py
@@ -487,15 +487,15 @@
             def _():
                 third_phase(DOWN)
                 gather2.step2()
+                complete(DOWN)
+                partial_out(act[1], wd, scatter2, row_set(1))
 
         with jax.named_scope("feed_down"):
             @pl.when(i == 3)
             def _():
+                scatter2.near()
                 gather2.step3()
-                complete(DOWN)
-                partial_out(act[1], wd, scatter2, row_set(1))
                 partial_out(act[2], wd, scatter2, row_set(2))
-                scatter2.near()
 
         with jax.named_scope("feed_from"):
             from_other(gather2, places)

time: 106 us -> 105 us (level)
  no operation moved by 1% of the time
where the time goes in v5:
time: 105 us
  Pallas kernels  104 us (99%)
    pallas_call x1, Pallas kernels, per_device(): pl.pallas_call(kernel, out_shape=pltpu.VMEM((128, 2048), F32), in_specs=[...  104 us

profile of v5, /device:TPU:1, one launch (start us, length us, event | category | flops | bytes accessed | tf_op | source)
XLA Modules:
  0.0 104.9 jit_solution(991088455062968860)
XLA Ops:
  0.0 104.0 %shard_map.145 = f32[128,2048]{1,0:T(8,128)S(1)} custom-call(bf16[128,2048]{1,0:T(8,128)(2,1)} %tokens_hbm.1, f32[16,64,128]{2,1,0:T(8,128)} %bitcast.13, bf16[4,32,128]{2,1,0:T(8,128)(2,1)} %bitcast.20, bf16[4,32,128]{2,1,0:T(8,128)(2,1)} %bitcast.21, bf16[4,32,256]{2,1,0:T(8,128)(2,1)} %bitcast.18, bf16[4,64,128]{2,1,0:T(8,128)(2,1)} %bitcast.19, ...), custom_call_target="tpu_custom_call" | custom-call | tf_op jit(solution)/shard_map/pallas_call | solution.py:548
  104.0 1.0 copy.17
